TPU v7x, 256 devices: a whole 4x4x8 slice. The times are simulated.
256 devices in a mesh: fs: 16 (over y, x), tp: 16 (over z, core).
Axes of the slice: x: 4, y: 4, z: 8, core: 2. Of those that a mesh axis runs over, the one named last changes fastest.
Arguments:
- tokens: bfloat16 [32768, 2048], P(('fs', 'tp')), may hold values from -6 to 6
- up_weight: bfloat16 [2048, 4096], P('fs', 'tp'), may hold values from -0.125 to 0.125
- down_weight: bfloat16 [4096, 2048], P('tp', 'fs'), may hold values from -0.09375 to 0.09375
- cotangent: bfloat16 [32768, 2048], P(('fs', 'tp')), may hold values from -24 to 24
Outputs:
- input_grad: bfloat16 [32768, 2048], P(('fs', 'tp'))
- up_grad: float32 [2048, 4096], P('fs', 'tp')
- down_grad: float32 [4096, 2048], P('tp', 'fs')
All inputs are finite; a program needn't handle non-finite values.
Results may differ from a plain program's by a relative error of at most 0.018.
Values may be sent and summed in bfloat16 or wider, within the bound.
A program may use at most 128 MiB of HBM per device.

v0:
```python
import jax
import jax.numpy as jnp
from jax import lax
from jax.sharding import PartitionSpec as P


def in_one_piece(arrays, axis, dim, along):
    ends, at = ([], 0)
    for a in arrays[:-1]:
        at += a.shape[along]
        ends.append(at)
    both = jnp.concatenate(arrays, axis=along)
    return tuple(jnp.split(lax.all_gather(both, axis, axis=dim, tiled=True), ends, axis=along))


def in_order(parts, dim):
    lengths = list(parts.shape[1:])
    lengths[dim] *= parts.shape[0]
    return jnp.moveaxis(parts, 0, dim).reshape(lengths)


def copy_for_each(value, axis):
    count = lax.axis_size(axis)
    return lax.all_to_all(
        jnp.broadcast_to(value[None], (count, *value.shape)), axis, 0, 0, tiled=True
    )


def gather_directly(value, axis, dim):
    return in_order(copy_for_each(value, axis), dim)


def cut_along(value, dim, count):
    before, after = (value.shape[:dim], value.shape[dim + 1 :])
    return jnp.moveaxis(value.reshape(*before, count, -1, *after), dim, 0)


def sent_and_summed(value, axis, dim):
    count = lax.axis_size(axis)
    parts = lax.all_to_all(cut_along(value, dim, count), axis, 0, 0, tiled=True)
    return jnp.sum(parts.astype(jnp.float32), axis=0)


def shards(tokens, up_weight, down_weight, cotangent):
    rows_all, cot_all = in_one_piece((tokens, cotangent), "tp", 0, 1)
    up_whole = gather_directly(up_weight, "fs", 0)
    pre = jnp.dot(rows_all, up_whole, preferred_element_type=jnp.float32)
    active = jnp.maximum(pre, 0.0)
    hidden = (active * active).astype(jnp.bfloat16)
    part = cot_all
    dhidden = lax.dot_general(
        part,
        gather_directly(down_weight, "fs", 1),
        (((1,), (1,)), ((), ())),
        preferred_element_type=jnp.float32,
    )
    dpre = (2.0 * active * dhidden).astype(jnp.bfloat16)
    count_all = tokens.shape[0] * lax.axis_size("fs") * lax.axis_size("tp")
    factor = 1.0 / jnp.sqrt(jnp.float32(count_all))
    part = rows_all
    up_grad = (
        sent_and_summed(
            lax.dot_general(
                part, dpre, (((0,), (0,)), ((), ())), preferred_element_type=jnp.float32
            ).astype(jnp.bfloat16),
            "fs",
            0,
        )
        * factor
    )
    down_term = lax.dot_general(
        hidden, cot_all, (((0,), (0,)), ((), ())), preferred_element_type=jnp.float32
    )
    down_grad = sent_and_summed(down_term.astype(jnp.bfloat16), "fs", 1) * factor
    part = dpre
    prod = lax.dot_general(
        part, up_whole, (((1,), (1,)), ((), ())), preferred_element_type=jnp.float32
    )
    rounded = lax.optimization_barrier(prod.astype(jnp.bfloat16))
    grad_rows = lax.psum_scatter(
        rounded.astype(jnp.float32).astype(jnp.bfloat16), "tp", scatter_dimension=0, tiled=True
    )
    return (grad_rows, up_grad, down_grad)


def solution(mesh):
    placed = (P(("fs", "tp"), None), P("fs", "tp"), P("tp", "fs"), P(("fs", "tp"), None))
    return jax.shard_map(
        shards,
        mesh=mesh,
        in_specs=placed,
        out_specs=(P(("fs", "tp"), None), P("fs", "tp"), P("tp", "fs")),
        check_vma=False,
    )
```

profile of v0, /device:TPU:4, one launch (start us, length us, event | category | flops | bytes accessed | tf_op | source)
XLA Modules:
  0.0 204.4 jit_solution(3619041158402113199)
XLA Ops:
  7.2 0.0 all-gather.2.cloned.1.call-start
  7.2 2.3 %pad_maximum_fusion = bf16[128,4096]{1,0:T(8,128)(2,1)} fusion(bf16[128,2048]{1,0:T(8,128)(2,1)} %param.7, bf16[128,2048]{1,0:T(8,128)(2,1)} %param.4), kind=kLoop, calls=%fused_computation.19 | loop fusion | flops 2097152 | bytes 2097152 | tf_op jit(solution)/shard_map/concatenate | solution.py:12
  9.5 0.0 all-gather.2.cloned.1.call-update
  9.5 2.0 broadcast_in_dim.4
  11.5 7.4 %all-to-all-start = ((bf16[16,128,256]{2,1,0:T(8,128)(2,1)}), bf16[16,128,256]{2,1,0:T(8,128)(2,1)S(1)}, u32[]{:S(2)}, u32[]{:S(2)}) async-start(bf16[16,128,256]{2,1,0:T(8,128)(2,1)} %broadcast_in_dim.4), calls=%async_computation | async-start | bytes 2097152 | tf_op jit(solution)/shard_map/all_to_all | solution.py:24
  18.9 0.9 copy.8
  19.9 13.6 %all-to-all-done = bf16[16,128,256]{2,1,0:T(8,128)(2,1)S(1)} async-done(((bf16[16,128,256]{2,1,0:T(8,128)(2,1)}), bf16[16,128,256]{2,1,0:T(8,128)(2,1)S(1)}, u32[]{:S(2)}, u32[]{:S(2)}) %all-to-all-start) | async-done | bytes 1048608 | tf_op jit(solution)/shard_map/all_to_all | solution.py:24
  33.5 1.1 broadcast_in_dim.5
  34.6 6.7 %all-to-all-start.1 = ((bf16[16,256,128]{1,2,0:T(8,128)(2,1)}), bf16[16,256,128]{1,2,0:T(8,128)(2,1)S(1)}, u32[]{:S(2)}, u32[]{:S(2)}) async-start(bf16[16,256,128]{1,2,0:T(8,128)(2,1)} %broadcast_in_dim.5), calls=%async_computation.1 | async-start | bytes 2097152 | tf_op jit(solution)/shard_map/all_to_all | solution.py:24
  41.3 0.0 reduce-scatter.2.cloned.1.call-start
  41.3 66.8 %all-gather.2.cloned.1.call-done = bf16[2048,4096]{1,0:T(8,128)(2,1)} async-done(((bf16[128,4096]{1,0:T(8,128)(2,1)}), bf16[2048,4096]{1,0:T(8,128)(2,1)}) %all-gather.2.cloned.1.call-update) | async-done | bytes 16777232 | tf_op jit(solution)/shard_map/all_gather | solution.py:13
  108.1 7.1 %fusion.8 = f32[2048,256]{1,0:T(8,128)} fusion(bf16[2048,256]{1,0:T(8,128)(2,1)S(1)} %bitcast.18, bf16[2048,4096]{1,0:T(8,128)(2,1)} %all-gather.2.cloned.1.call-done), kind=kOutput, calls=%fused_computation.9 | convolution fusion | flops 2148007936 | bytes 11534336 | tf_op jit(solution)/shard_map/dot_general | solution.py:47
  115.2 0.0 all-to-all-done.1
  115.2 6.4 %fusion.14 = bf16[2048,256]{1,0:T(8,128)(2,1)S(1)} fusion(bf16[256,2048]{0,1:T(8,128)(2,1)S(1)} %bitcast.20, bf16[2048,4096]{1,0:T(8,128)(2,1)} %all-gather.2.cloned.1.call-done, f32[2048,256]{1,0:T(8,128)} %fusion.8), kind=kOutput, calls=%fused_computation.11 | convolution fusion | flops 2149056512 | bytes 12582912 | tf_op jit(solution)/shard_map/dot_general | solution.py:51
  121.6 5.6 %convolution_convert_fusion = bf16[2048,2048]{1,0:T(8,128)(2,1)} fusion(bf16[2048,256]{1,0:T(8,128)(2,1)S(1)} %fusion.14, bf16[2048,256]{1,0:T(8,128)(2,1)S(1)} %bitcast.19), kind=kOutput, calls=%fused_computation | convolution fusion | flops 2151677952 | bytes 10485760 | tf_op jit(solution)/shard_map/dot_general | solution.py:76
  127.2 0.0 copy-start
  127.2 0.0 reduce-scatter.2.cloned.1.call-update
  127.2 1.6 copy-done
  128.8 5.7 %fusion.23 = bf16[32,16,8,128]{3,2,1,0:T(8,128)(2,1)S(1)} fusion(bf16[2048,4096]{1,0:T(8,128)(2,1)} %all-gather.2.cloned.1.call-done, f32[2048,256]{1,0:T(8,128)S(1)} %copy-done), kind=kOutput, calls=%fused_computation.17 | convolution fusion | flops 2149056512 | bytes 11534336 | tf_op jit(solution)/shard_map/dot_general | solution.py:71
  134.5 1.2 copy.12
  135.7 7.3 %all-to-all-start.3 = ((bf16[16,256,128]{2,1,0:T(8,128)(2,1)}), bf16[16,256,128]{2,1,0:T(8,128)(2,1)S(1)}, u32[]{:S(2)}, u32[]{:S(2)}) async-start(bf16[16,256,128]{2,1,0:T(8,128)(2,1)} %bitcast.17), calls=%async_computation.4 | async-start | bytes 2097152 | tf_op jit(solution)/shard_map/all_to_all | solution.py:40
  143.0 7.1 %fusion.17 = bf16[2048,256]{1,0:T(8,128)(2,1)} fusion(bf16[2048,256]{1,0:T(8,128)(2,1)S(1)} %fusion.14, bf16[2048,4096]{1,0:T(8,128)(2,1)} %all-gather.2.cloned.1.call-done), kind=kOutput, calls=%fused_computation.12 | convolution fusion | flops 2148007936 | bytes 10485760 | tf_op jit(solution)/shard_map/dot_general | solution.py:63
  150.1 7.8 %all-to-all-done.3 = bf16[16,256,128]{2,1,0:T(8,128)(2,1)S(1)} async-done(((bf16[16,256,128]{2,1,0:T(8,128)(2,1)}), bf16[16,256,128]{2,1,0:T(8,128)(2,1)S(1)}, u32[]{:S(2)}, u32[]{:S(2)}) %all-to-all-start.3) | async-done | bytes 1048608 | tf_op jit(solution)/shard_map/all_to_all | solution.py:40
  157.9 6.5 %all-to-all-start.2 = ((bf16[16,128,256]{2,1,0:T(8,128)(2,1)}), bf16[16,128,256]{2,1,0:T(8,128)(2,1)S(1)}, u32[]{:S(2)}, u32[]{:S(2)}) async-start(bf16[16,128,256]{2,1,0:T(8,128)(2,1)} %bitcast.3), calls=%async_computation.3 | async-start | bytes 2097152 | tf_op jit(solution)/shard_map/all_to_all | solution.py:40
  164.4 0.1 convert_reduce_fusion
  164.6 14.5 %all-to-all-done.2 = bf16[16,128,256]{2,1,0:T(8,128)(2,1)S(1)} async-done(((bf16[16,128,256]{2,1,0:T(8,128)(2,1)}), bf16[16,128,256]{2,1,0:T(8,128)(2,1)S(1)}, u32[]{:S(2)}, u32[]{:S(2)}) %all-to-all-start.2) | async-done | bytes 1048608 | tf_op jit(solution)/shard_map/all_to_all | solution.py:40
  179.0 0.1 convert_reduce_fusion.1
  179.2 0.7 broadcast_multiply_fusion
  179.8 0.7 broadcast_multiply_fusion.1
  180.5 17.0 %reduce-scatter.2.cloned.1.call-done = bf16[128,2048]{1,0:T(8,128)(2,1)} async-done(((bf16[2048,2048]{1,0:T(8,128)(2,1)}), bf16[128,2048]{1,0:T(8,128)(2,1)}) %reduce-scatter.2.cloned.1.call-update) | async-done | bytes 524304 | tf_op jit(solution)/shard_map/reduce_scatter | solution.py:80
Async XLA Ops:
  7.2 100.9 %all-gather.2.cloned.1.call-start = ((), (), s32[]{:S(2)}) async-start(), calls=%async_computation.5 | async-start | bytes 17825792 | tf_op jit(solution)/shard_map/all_gather | solution.py:13
  11.5 22.0 %all-to-all-start = ((bf16[16,128,256]{2,1,0:T(8,128)(2,1)}), bf16[16,128,256]{2,1,0:T(8,128)(2,1)S(1)}, u32[]{:S(2)}, u32[]{:S(2)}) async-start(bf16[16,128,256]{2,1,0:T(8,128)(2,1)} %broadcast_in_dim.4), calls=%async_computation | async-start | bytes 2097152 | tf_op jit(solution)/shard_map/all_to_all | solution.py:24
  34.6 80.6 %all-to-all-start.1 = ((bf16[16,256,128]{1,2,0:T(8,128)(2,1)}), bf16[16,256,128]{1,2,0:T(8,128)(2,1)S(1)}, u32[]{:S(2)}, u32[]{:S(2)}) async-start(bf16[16,256,128]{1,2,0:T(8,128)(2,1)} %broadcast_in_dim.5), calls=%async_computation.1 | async-start | bytes 2097152 | tf_op jit(solution)/shard_map/all_to_all | solution.py:24
  41.3 156.2 %reduce-scatter.2.cloned.1.call-start = ((), (), s32[]{:S(2)}) async-start(), calls=%async_computation.6 | async-start | bytes 8912896 | tf_op jit(solution)/shard_map/reduce_scatter | solution.py:80
  127.2 1.6 copy-start
  135.7 22.2 %all-to-all-start.3 = ((bf16[16,256,128]{2,1,0:T(8,128)(2,1)}), bf16[16,256,128]{2,1,0:T(8,128)(2,1)S(1)}, u32[]{:S(2)}, u32[]{:S(2)}) async-start(bf16[16,256,128]{2,1,0:T(8,128)(2,1)} %bitcast.17), calls=%async_computation.4 | async-start | bytes 2097152 | tf_op jit(solution)/shard_map/all_to_all | solution.py:40
  157.9 21.1 %all-to-all-start.2 = ((bf16[16,128,256]{2,1,0:T(8,128)(2,1)}), bf16[16,128,256]{2,1,0:T(8,128)(2,1)S(1)}, u32[]{:S(2)}, u32[]{:S(2)}) async-start(bf16[16,128,256]{2,1,0:T(8,128)(2,1)} %bitcast.3), calls=%async_computation.3 | async-start | bytes 2097152 | tf_op jit(solution)/shard_map/all_to_all | solution.py:40
Sparse Core Ops, SparseCore 0:
  9.8 98.2 all-gather.1
  127.3 70.1 reduce-scatter.1
where the time goes:
time: 205 us; the launch traced here: 204 us
  waiting for transfers between devices  120 us (59%)
  matrix products  31.9 us (16%)
  starting transfers between devices  27.9 us (14%)
  between operations  14.1 us (7%)
  local copies, waits for them, and re-layouts  6.86 us (3%)
  other arithmetic  3.89 us (2%)
    all_gather x1, waiting for transfers between devices, in_one_piece(): lax.all_gather(both, axis, axis=dim, tiled=True)  66.8 us
    all_to_all x2, waiting for transfers between devices, sent_and_summed(): parts = lax.all_to_all(cut_along(value, dim, count), axis, 0, 0, tiled=True)  22.3 us
    reduce_scatter x1, waiting for transfers between devices, shards(): lax.psum_scatter(rounded.astype(jnp.float32).astype(jnp.bfloat16), 'tp',...  17 us
    all_to_all x2, starting transfers between devices, copy_for_each(): lax.all_to_all(jnp.broadcast_to(value[None], (count, *value.shape)), axis...  14.1 us
    all_to_all x2, starting transfers between devices, sent_and_summed(): parts = lax.all_to_all(cut_along(value, dim, count), axis, 0, 0, tiled=True)  13.7 us
    all_to_all x2, waiting for transfers between devices, copy_for_each(): lax.all_to_all(jnp.broadcast_to(value[None], (count, *value.shape)), axis...  13.6 us
    dot_general x1, matrix products, shards(): lax.dot_general(part, dpre, (((0,), (0,)), ((), ())), preferred_element_t...  7.13 us
    dot_general x1, matrix products, shards(): pre = jnp.dot(rows_all, up_whole, preferred_element_type=jnp.float32)  7.09 us
  transfers between devices with their start and end apart: 6, of which 5 were waited for; matrix products, arithmetic and copies ran while one was open for 13% of the time, Pallas kernels for 0%

commit v1 on v0

v1 whole, which is shorter than its diff:
```python
import jax
import jax.numpy as jnp
from jax import lax
from jax.experimental import pallas as pl
from jax.experimental.pallas import tpu as pltpu
from jax.sharding import PartitionSpec as P

BF = jnp.bfloat16
F32 = jnp.float32
MESH = pl.DeviceIdType.MESH

SX, ZP, ZM, YP, YM, YF = 0, 8, 16, 24, 40, 56
TP, TM, TF, TC = 60, 62, 64, 66
GY, GC, GA, GB, FS = 74, 82, 98, 106, 114
XC, XY = 116, 118
FSS = 124
N_SEM = 132


def both(n, body):
    def step(i, carry):
        body(i)
        return carry

    lax.fori_loop(0, n, step, 0)


def kernel(
    factor, tok_in, up_in, dn_in, cot_in, ig_out, ug_out, dg_out,
    X, WS, W, DP, TT, G, RY, RC, ZA, ZB, FX, S, RP, XR, ssem, rsem, lsem,
):
    fs, tp = lax.axis_index("fs"), lax.axis_index("tp")
    y, x = fs // 4, fs % 4
    z, c = tp // 2, tp % 2
    p = lax.rem(z - x + 8, 4)
    xp, xm, xo = (x + 1) % 4, (x + 3) % 4, (x + 2) % 4
    yp, ym, yo = (y + 1) % 4, (y + 3) % 4, (y + 2) % 4
    zp, zm = (z + 1) % 8, (z + 7) % 8

    def dev(yy, xx, zz, cc):
        return (yy * 4 + xx, zz * 2 + cc)

    XP, XM, XO = dev(y, xp, z, c), dev(y, xm, z, c), dev(y, xo, z, c)
    YPd, YMd = dev(yp, x, z, c), dev(ym, x, z, c)
    ZPd, ZMd = dev(y, x, zp, c), dev(y, x, zm, c)
    PA = dev(y, x, z, 1 - c)

    def copy(src, dst, to, sid, sent_id=None):
        sent_id = sid if sent_id is None else sent_id
        return pltpu.make_async_remote_copy(
            src_ref=src, dst_ref=dst, send_sem=ssem.at[sent_id], recv_sem=rsem.at[sid],
            device_id=to, device_id_type=MESH,
        )

    def got(ref, sid):
        copy(ref, ref, PA, sid).wait_recv()

    def sent(ref, sid):
        copy(ref, ref, PA, sid).wait_send()

    crow = pl.ds(pl.multiple_of(c * 128, 128), 128)
    own = [pltpu.make_async_copy(a, X.at[w, x, crow, :], lsem.at[w]) for w, a in enumerate((tok_in, cot_in))]
    for o in own:
        o.start()
    WS[0] = up_in[...]
    WS[1] = dn_in[...].astype(F32).T.astype(BF)

    barrier = pltpu.get_barrier_semaphore()
    for to in (XP, XM, XO, YPd, YMd, ZPd, ZMd, PA):
        pl.semaphore_signal(barrier, inc=1, device_id=to, device_id_type=MESH)
    pl.semaphore_wait(barrier, 8)

    def wrow(yy, j):
        return pl.ds(pl.multiple_of(yy * 512 + j * 128, 128), 128)

    def wpiece(slot, w, yy, j):
        return W.at[slot, w, wrow(yy, j), :]

    @pl.when(p != 0)
    def _():
        for w in range(2):
            copy(WS.at[w], wpiece(0, w, y, x), dev(y, (x + p) % 4, z, c), SX + w * 4 + x).start()

    for o in own:
        o.wait()

    def xblock(w, xx, cc_row):
        return X.at[w, xx, cc_row, :]

    for w, to, base in ((0, XP, TP), (1, XM, TM), (1, XP, TP), (0, XM, TM)):
        copy(xblock(w, x, crow), xblock(w, x, crow), to, base + w).start()
    for w in range(2):
        copy(xblock(w, x, crow), xblock(w, x, crow), PA, TC + w * 4).start()

    @pl.when(p == 0)
    def _():
        for w in range(2):
            W[0, w, wrow(y, x), :] = WS[w]

    def ysend(slot, k, w, j):
        piece = wpiece(slot, w, y, j)
        copy(piece, piece, YPd, YP + slot * 8 + k).start()
        copy(piece, piece, YMd, YM + slot * 8 + k).start()

    def step_a(k):
        w, j = k // 4, k % 4

        @pl.when((p == 0) & (j != x))
        def _():
            got(wpiece(0, w, y, j), SX + k)

        @pl.when(p != 0)
        def _():
            got(wpiece(0, w, y, j), ZP + k)

        copy(wpiece(0, w, y, j), wpiece(jnp.where(p == 3, 1, 0), w, y, j), ZPd, ZP + k).start()

        @pl.when(p == 0)
        def _():
            copy(wpiece(0, w, y, j), wpiece(1, w, y, j), ZMd, ZM + k).start()

        ysend(0, k, w, j)

    def step_b(k):
        w, j = k // 4, k % 4

        @pl.when(p == 0)
        def _():
            got(wpiece(1, w, y, j), ZP + k)

        @pl.when(p != 0)
        def _():
            got(wpiece(1, w, y, j), ZM + k)

        @pl.when(p >= 2)
        def _():
            copy(wpiece(1, w, y, j), wpiece(1, w, y, j), ZMd, ZM + k).start()

        ysend(1, k, w, j)

    lag_a = jnp.where(p == 3, 5, 0)
    lag_b = jnp.where(p == 0, 8, jnp.where(p == 1, 5, 0))

    def zstep(t):
        @pl.when((t >= lag_a) & (t < lag_a + 8))
        def _():
            step_a(t - lag_a)

        @pl.when((t >= lag_b) & (t < lag_b + 8))
        def _():
            step_b(t - lag_b)

    both(8, zstep)
    got(xblock(0, xm, crow), TP)
    copy(xblock(0, xm, crow), xblock(0, xm, crow), XP, TF).start()
    got(xblock(1, xp, crow), TM + 1)
    copy(xblock(1, xp, crow), xblock(1, xp, crow), XM, TF + 1).start()
    both(8, lambda t: zstep(t + 8))

    def wblock(slot, w, yy):
        return W.at[slot, w, pl.ds(pl.multiple_of(yy * 512, 512), 512), :]

    near = jnp.where(p == 3, 1, 0)

    def yforward(i):
        slot = jnp.where(i == 0, near, 1 - near)

        def up(k):
            got(wpiece(slot, 0, ym, k), YP + slot * 8 + k)

        both(4, up)
        copy(wblock(slot, 0, ym), wblock(slot, 0, ym), YPd, YF + slot * 2).start()

        def dn(k):
            got(wpiece(slot, 1, yp, k), YM + slot * 8 + 4 + k)

        both(4, dn)
        copy(wblock(slot, 1, yp), wblock(slot, 1, yp), YMd, YF + slot * 2 + 1).start()

    both(2, yforward)

    def pass_on(w, r):
        xx = (x + r) % 4
        copy(xblock(w, xx, crow), xblock(w, xx, crow), PA, TC + w * 4 + r).start()

    pass_on(0, 3)
    pass_on(1, 1)
    got(xblock(1, xm, crow), TP + 1)
    pass_on(1, 3)
    got(xblock(0, xp, crow), TM)
    pass_on(0, 1)
    got(xblock(0, xo, crow), TF)
    pass_on(0, 2)
    got(xblock(1, xo, crow), TF + 1)
    pass_on(1, 2)

    def yfinish(slot):
        def up(k):
            got(wpiece(slot, 0, yp, k), YM + slot * 8 + k)
            got(wpiece(slot, 1, ym, k), YP + slot * 8 + 4 + k)

        both(4, up)
        for w in range(2):
            got(wblock(slot, w, yo), YF + slot * 2 + w)

    both(2, yfinish)
    orow = pl.ds(pl.multiple_of((1 - c) * 128, 128), 128)
    for w in range(2):
        both(4, lambda r, w=w: got(xblock(w, (x + r) % 4, orow), TC + w * 4 + r))

    def act(i):
        slot, xx = i // 4, i % 4
        pre = jnp.dot(X[0, xx], W[slot, 0], preferred_element_type=F32)
        dh = jnp.dot(X[1, xx], W[slot, 1], preferred_element_type=F32)
        active = jnp.maximum(pre, 0.0)
        hidden = active * active
        dpre = 2.0 * active * dh
        DP[slot, pl.ds(pl.multiple_of(xx * 256, 256), 256), :] = dpre.astype(BF)
        cols = pl.ds(pl.multiple_of(xx * 256, 256), 256)
        TT[slot, 0, :, cols] = dpre.T.astype(BF)
        TT[slot, 1, :, cols] = hidden.T.astype(BF)

    both(8, act)

    first = jnp.where(p < 2, 1, 0)

    def grads(slot):
        def block(i):
            yy = (y + 2 + i) % 4
            cols = pl.ds(pl.multiple_of(yy * 512, 512), 512)
            for w in range(2):
                rows = X[w, :, :, cols].reshape(1024, 512)
                part = jnp.dot(TT[slot, w], rows, preferred_element_type=F32).astype(BF)
                for j in range(4):
                    G[slot, w, yy, j] = part[:, j * 128 : (j + 1) * 128]

        both(4, block)

    def ab(slot):
        base = GY + slot * 4
        copy(G.at[slot, 0, yo], RY.at[slot, 0, 0], YPd, base).start()
        copy(G.at[slot, 1, yo], RY.at[slot, 1, 0], YMd, base + 1).start()
        copy(G.at[slot, 1, yp], RY.at[slot, 0, 1], YPd, base + 2).start()
        copy(G.at[slot, 0, ym], RY.at[slot, 1, 1], YMd, base + 3).start()

    def cstep(slot):
        base = GY + slot * 4
        got(RY.at[slot, 0, 0], base)
        got(RY.at[slot, 1, 0], base + 1)

        def piece(j):
            G[slot, 0, yp, j] = (G[slot, 0, yp, j].astype(F32) + RY[slot, 0, 0, j].astype(F32)).astype(BF)
            copy(G.at[slot, 0, yp, j], RC.at[slot, 0, j], YPd, GC + slot * 8 + j).start()
            G[slot, 1, ym, j] = (G[slot, 1, ym, j].astype(F32) + RY[slot, 1, 0, j].astype(F32)).astype(BF)
            copy(G.at[slot, 1, ym, j], RC.at[slot, 1, j], YMd, GC + slot * 8 + 4 + j).start()

        both(4, piece)

    def yfinal(slot):
        base = GY + slot * 4
        got(RY.at[slot, 0, 1], base + 2)
        got(RY.at[slot, 1, 1], base + 3)

        def piece(j):
            got(RC.at[slot, 0, j], GC + slot * 8 + j)
            G[slot, 0, y, j] = (
                G[slot, 0, y, j].astype(F32) + RC[slot, 0, j].astype(F32) + RY[slot, 1, 1, j].astype(F32)
            ).astype(BF)
            got(RC.at[slot, 1, j], GC + slot * 8 + 4 + j)
            G[slot, 1, y, j] = (
                G[slot, 1, y, j].astype(F32) + RC[slot, 1, j].astype(F32) + RY[slot, 0, 1, j].astype(F32)
            ).astype(BF)

        both(4, piece)

    grads(first)
    ab(first)
    grads(1 - first)

    def igrad(n):
        rows = pl.ds(pl.multiple_of(n * 256, 256), 256)
        nt = (((1,), (1,)), ((), ()))
        part = lax.dot_general(DP[0], W[0, 0, rows, :], nt, preferred_element_type=F32)
        part = part + lax.dot_general(DP[1], W[1, 0, rows, :], nt, preferred_element_type=F32)
        part = part.astype(BF).reshape(4, 2, 128, 256)
        cols = pl.ds(pl.multiple_of((n % 4) * 256, 256), 256)
        for cc in range(2):
            S[cc, n // 4, :, :, cols] = part[:, cc]

    for half in range(2):
        both(4, lambda n, half=half: igrad(half * 4 + n))
        copy(S.at[1 - c, half], RP.at[half], PA, XC + half).start()

    cstep(first)
    ab(1 - first)

    for half in range(2):
        got(RP.at[half], XC + half)

        def add(r, half=half):
            S[c, half, r] = (S[c, half, r].astype(F32) + RP[half, r].astype(F32)).astype(BF)

        both(4, add)
    copy(S.at[c, 0, xo], XR.at[0, 0], XP, XY).start()
    copy(S.at[c, 1, xo], XR.at[1, 0], XM, XY + 1).start()
    copy(S.at[c, 1, xp], XR.at[0, 1], XP, XY + 2).start()
    copy(S.at[c, 0, xm], XR.at[1, 1], XM, XY + 3).start()

    def gpiece(slot, k):
        return G.at[slot, k // 4, y, k % 4]

    def chain_b(k):
        w, j = k // 4, k % 4

        @pl.when(p == 0)
        def _():
            copy(gpiece(1, k), ZA.at[k], ZMd, GA + k).start()

        @pl.when(p >= 2)
        def _():
            got(ZB.at[k], GB + k)
            G[1, w, y, j] = (G[1, w, y, j].astype(F32) + ZB[k].astype(F32)).astype(BF)

        @pl.when(p != 0)
        def _():
            copy(gpiece(1, k), ZB.at[k], ZPd, GB + k).start()

    def chain_a(k):
        w, j = k // 4, k % 4
        got(ZA.at[k], GA + k)

        @pl.when(p != 0)
        def _():
            G[0, w, y, j] = (G[0, w, y, j].astype(F32) + ZA[k].astype(F32)).astype(BF)
            copy(gpiece(0, k), ZA.at[k], ZMd, GA + k).start()

        @pl.when(p == 0)
        def _():
            got(ZB.at[k], GB + k)
            G[0, w, y, j] = (G[0, w, y, j].astype(F32) + ZA[k].astype(F32) + ZB[k].astype(F32)).astype(BF)

            @pl.when(j != x)
            def _():
                copy(gpiece(0, k), FX.at[w], dev(y, j, z, c), FS + w, FSS + k).start()

    def order(k):
        return (k % 2) * 4 + k // 2

    yfinal(first)

    @pl.when(p < 2)
    def _():
        both(8, lambda k: chain_b(order(k)))

    cstep(1 - first)

    @pl.when(p >= 2)
    def _():
        both(8, lambda k: chain_a(order(k)))

    got(XR.at[0, 0], XY)
    S[c, 0, xp] = (S[c, 0, xp].astype(F32) + XR[0, 0].astype(F32)).astype(BF)
    copy(S.at[c, 0, xp], XR.at[0, 2], XP, XY + 4).start()
    got(XR.at[1, 0], XY + 1)
    S[c, 1, xm] = (S[c, 1, xm].astype(F32) + XR[1, 0].astype(F32)).astype(BF)
    copy(S.at[c, 1, xm], XR.at[1, 2], XM, XY + 5).start()

    yfinal(1 - first)

    @pl.when(p < 2)
    def _():
        both(8, lambda k: chain_a(order(k)))

    @pl.when(p >= 2)
    def _():
        both(8, lambda k: chain_b(order(k)))

    got(XR.at[0, 1], XY + 2)
    got(XR.at[1, 1], XY + 3)
    got(XR.at[0, 2], XY + 4)
    got(XR.at[1, 2], XY + 5)
    for half, (d0, k0), (d1, k1) in ((0, (0, 2), (1, 1)), (1, (0, 1), (1, 2))):
        ig_out[:, half * 1024 : (half + 1) * 1024] = (
            S[c, half, x].astype(F32) + XR[d0, k0].astype(F32) + XR[d1, k1].astype(F32)
        ).astype(BF)

    @pl.when(p == 0)
    def _():
        for w in range(2):
            FX[w] = G[0, w, y, x]

    @pl.when(p != 0)
    def _():
        for w in range(2):
            got(FX.at[w], FS + w)

    ug_out[...] = FX[0].astype(F32).T * factor
    dg_out[...] = FX[1].astype(F32) * factor

    @pl.when(p != 0)
    def _():
        for w in range(2):
            sent(WS.at[w], SX + w * 4 + x)

    def sends(k):
        w, j = k // 4, k % 4
        piece = wpiece(0, w, y, j)
        sent(piece, ZP + k)

        @pl.when(p != 1)
        def _():
            sent(piece, ZM + k)

        for slot in range(2):
            sent(wpiece(slot, w, y, j), YP + slot * 8 + k)
            sent(wpiece(slot, w, y, j), YM + slot * 8 + k)
        sent(ZA.at[k], GA + k)

        @pl.when(p != 0)
        def _():
            sent(ZB.at[k], GB + k)

        @pl.when((p == 0) & (j != x))
        def _():
            sent(FX.at[w], FSS + k)

        both(2, lambda slot: sent(G.at[slot, w, y, j], GC + slot * 8 + k))
        sent(xblock(w, x, crow), TC + k)

    both(8, sends)
    for i in range(4):
        sent(wblock(0, 0, y), YF + i)
    for i in range(6):
        sent(xblock(0, x, crow), TP + i)
    for i in range(8):
        sent(G.at[0, 0, y], GY + i)
    for i in range(2):
        sent(S.at[0, 0], XC + i)
    for i in range(6):
        sent(S.at[0, 0, 0], XY + i)


def solution(mesh):
    def shards(tokens, up_weight, down_weight, cotangent):
        count_all = tokens.shape[0] * lax.axis_size("fs") * lax.axis_size("tp")
        factor = 1.0 / float(count_all) ** 0.5
        vmem = pl.BlockSpec(memory_space=pltpu.VMEM)
        hbm = pl.BlockSpec(memory_space=pl.ANY)

        def body(*refs):
            kernel(factor, *refs)

        return pl.pallas_call(
            body,
            out_shape=(
                jax.ShapeDtypeStruct((128, 2048), BF),
                jax.ShapeDtypeStruct((128, 256), F32),
                jax.ShapeDtypeStruct((256, 128), F32),
            ),
            in_specs=[hbm, vmem, vmem, hbm],
            out_specs=(vmem, vmem, vmem),
            scratch_shapes=[
                pltpu.VMEM((2, 4, 256, 2048), BF),
                pltpu.VMEM((2, 128, 256), BF),
                pltpu.VMEM((2, 2, 2048, 256), BF),
                pltpu.VMEM((2, 1024, 256), BF),
                pltpu.VMEM((2, 2, 256, 1024), BF),
                pltpu.VMEM((2, 2, 4, 4, 256, 128), BF),
                pltpu.VMEM((2, 2, 2, 4, 256, 128), BF),
                pltpu.VMEM((2, 2, 4, 256, 128), BF),
                pltpu.VMEM((8, 256, 128), BF),
                pltpu.VMEM((8, 256, 128), BF),
                pltpu.VMEM((2, 256, 128), BF),
                pltpu.VMEM((2, 2, 4, 128, 1024), BF),
                pltpu.VMEM((2, 4, 128, 1024), BF),
                pltpu.VMEM((2, 3, 128, 1024), BF),
                pltpu.SemaphoreType.DMA((N_SEM,)),
                pltpu.SemaphoreType.DMA((N_SEM,)),
                pltpu.SemaphoreType.DMA((2,)),
            ],
            compiler_params=pltpu.CompilerParams(
                collective_id=0, has_side_effects=True, vmem_limit_bytes=60 * 2**20
            ),
            name="ffn_backward",
        )(tokens, up_weight, down_weight, cotangent)

    placed = (P(("fs", "tp"), None), P("fs", "tp"), P("tp", "fs"), P(("fs", "tp"), None))
    return jax.shard_map(
        shards,
        mesh=mesh,
        in_specs=placed,
        out_specs=(P(("fs", "tp"), None), P("fs", "tp"), P("tp", "fs")),
        check_vma=False,
    )
```

time: 205 us -> 128 us (0.62)
  Pallas kernels: 0 us -> 122 us
  waiting for transfers between devices: 120 us -> 0 us
  matrix products: 31.9 us -> 0 us
  starting transfers between devices: 27.9 us -> 0 us
  between operations: 14.1 us -> 0.65 us
  other arithmetic: 3.89 us -> 0 us
  local copies, waits for them, and re-layouts: 6.86 us -> 3.53 us
    pallas_call x0 -> x1, Pallas kernels: none -> 122 us  [shards(): pl.pallas_call(body, out_shape=(jax.ShapeDtypeStruct((128, 2048), BF), ja...]
    all_gather x1 -> x0, waiting for transfers between devices: 66.8 us -> none  [in_one_piece(): lax.all_gather(both, axis, axis=dim, tiled=True)]
    all_to_all x4 -> x0, waiting for transfers between devices: 35.9 us -> none  [the longest x2 22.3 us: sent_and_summed(): parts = lax.all_to_all(cut_along(value, dim, count), axis, 0, 0, tiled=True)]
    dot_general x5 -> x0, matrix products: 31.9 us -> none  [the longest x1 7.13 us: shards(): lax.dot_general(part, dpre, (((0,), (0,)), ((), ())), preferred_element_t...]
    all_to_all x4 -> x0, starting transfers between devices: 27.9 us -> none  [the longest x2 14.1 us: copy_for_each(): lax.all_to_all(jnp.broadcast_to(value[None], (count, *value.shape)), axis...]
    reduce_scatter x1 -> x0, waiting for transfers between devices: 17 us -> none  [shards(): lax.psum_scatter(rounded.astype(jnp.float32).astype(jnp.bfloat16), 'tp',...]
    broadcast_in_dim x2 -> x0, local copies, waits for them, and re-layouts: 3.12 us -> none  [copy_for_each(): jnp.broadcast_to(value[None], (count, *value.shape))]
    concatenate x1 -> x0, other arithmetic: 2.27 us -> none  [in_one_piece(): both = jnp.concatenate(arrays, axis=along)]
  transfers between devices with their start and end apart: 6 -> 0, of which waited for: 5 -> 0; matrix products, arithmetic and copies ran while one was open for 13% -> 0% of each run, Pallas kernels for 0% -> 0%
where the time goes in v1:
time: 128 us; the launch traced here: 126 us
  Pallas kernels  122 us (95%)
  local copies, waits for them, and re-layouts  3.53 us (3%)
    pallas_call x1, Pallas kernels, shards(): pl.pallas_call(body, out_shape=(jax.ShapeDtypeStruct((128, 2048), BF), ja...  122 us
    unnamed x7, local copies, waits for them, and re-layouts  3.53 us

profile of v1, /device:TPU:4, one launch (start us, length us, event | category | flops | bytes accessed | tf_op | source)
XLA Modules:
  0.0 126.1 jit_solution(15266400084090966486)
XLA Ops:
  0.6 122.0 %ffn_backward.1 = (bf16[128,2048]{1,0:T(8,128)(2,1)}, f32[128,256]{1,0:T(8,128)}, f32[256,128]{1,0:T(8,128)}) custom-call(bf16[128,2048]{1,0:T(8,128)(2,1)} %refs_0_.1, bf16[128,256]{1,0:T(8,128)(2,1)} %refs_1_.1, bf16[256,128]{1,0:T(8,128)(2,1)} %refs_2_.1, bf16[128,2048]{1,0:T(8,128)(2,1)} %refs_3_.1), custom_call_target="tpu_custom_call" | custom-call | tf_op jit(solution)/shard_map/ffn_backward/pallas_call | solution.py:453
  122.6 0.0 copy-start.1
  122.6 1.9 %copy.10 = bf16[128,2048]{1,0:T(8,128)(2,1)} copy(bf16[128,2048]{1,0:T(8,128)(2,1)} %get-tuple-element.6) | data formatting | bytes 1048576
  124.5 0.0 copy-done.1
  124.5 0.0 copy-start
  124.5 0.7 copy.11
  125.2 0.3 copy-done
  125.5 0.7 copy.12
Async XLA Ops:
  122.6 1.9 %copy-start.1 = (f32[128,256]{1,0:T(8,128)S(1)}, f32[128,256]{1,0:T(8,128)}, u32[]{:S(2)}) copy-start(f32[128,256]{1,0:T(8,128)} %get-tuple-element.7) | copy-start | bytes 393220
  124.5 1.0 copy-start

commit v2 on v1

v2 whole, which is shorter than its diff:
```python
import jax
import jax.numpy as jnp
from jax import lax
from jax.experimental import pallas as pl
from jax.experimental.pallas import tpu as pltpu
from jax.sharding import PartitionSpec as P

BF = jnp.bfloat16
F32 = jnp.float32
MESH = pl.DeviceIdType.MESH

SX, ZP, ZM, YP, YM, YF = 0, 8, 22, 36, 52, 68
TP, TM, TF, TC = 84, 86, 88, 90
GY, GC, GA, GB, QA, QB, RS = 98, 106, 118, 124, 130, 138, 146
FS, FSS, XC, XY = 152, 154, 162, 164
N_SEM = 170


def both(n, body):
    def step(i, carry):
        body(i)
        return carry

    lax.fori_loop(0, n, step, 0)


def kernel(
    factor, tok_in, up_in, dn_in, cot_in, ig_out, ug_out, dg_out,
    X, WS, W, DP, TT, G, RY, RC, ZA, ZB, UA, UB, RG, FX, S, RP, XR, ssem, rsem, lsem,
):
    fs, tp = lax.axis_index("fs"), lax.axis_index("tp")
    y, x = fs // 4, fs % 4
    z, c = tp // 2, tp % 2
    p = lax.rem(z - x + 8, 4)
    xp, xm, xo = (x + 1) % 4, (x + 3) % 4, (x + 2) % 4
    yp, ym, yo = (y + 1) % 4, (y + 3) % 4, (y + 2) % 4
    zp, zm = (z + 1) % 8, (z + 7) % 8

    def dev(yy, xx, zz, cc):
        return (yy * 4 + xx, zz * 2 + cc)

    XP, XM, XO = dev(y, xp, z, c), dev(y, xm, z, c), dev(y, xo, z, c)
    YPd, YMd = dev(yp, x, z, c), dev(ym, x, z, c)
    ZPd, ZMd = dev(y, x, zp, c), dev(y, x, zm, c)
    PA = dev(y, x, z, 1 - c)

    def copy(src, dst, to, sid, sent_id=None):
        sent_id = sid if sent_id is None else sent_id
        return pltpu.make_async_remote_copy(
            src_ref=src, dst_ref=dst, send_sem=ssem.at[sent_id], recv_sem=rsem.at[sid],
            device_id=to, device_id_type=MESH,
        )

    def got(ref, sid):
        copy(ref, ref, PA, sid).wait_recv()

    def sent(ref, sid):
        copy(ref, ref, PA, sid).wait_send()

    crow = pl.ds(pl.multiple_of(c * 128, 128), 128)
    own = [pltpu.make_async_copy(a, X.at[w, x, crow, :], lsem.at[w]) for w, a in enumerate((tok_in, cot_in))]
    for o in own:
        o.start()
    WS[0] = up_in[...]
    WS[1] = dn_in[...].astype(F32).T.astype(BF)

    barrier = pltpu.get_barrier_semaphore()
    for to in (XP, XM, XO, YPd, YMd, ZPd, ZMd, PA):
        pl.semaphore_signal(barrier, inc=1, device_id=to, device_id_type=MESH)
    pl.semaphore_wait(barrier, 8)

    def wrow(yy, j):
        return pl.ds(pl.multiple_of(yy * 512 + j * 128, 128), 128)

    def wpiece(slot, w, yy, j):
        return W.at[slot, w, wrow(yy, j), :]

    @pl.when(p != 0)
    def _():
        for w in range(2):
            copy(WS.at[w], wpiece(0, w, y, x), dev(y, (x + p) % 4, z, c), SX + w * 4 + x).start()

    for o in own:
        o.wait()

    def xblock(w, xx, cc_row):
        return X.at[w, xx, cc_row, :]

    for w, to, base in ((0, XP, TP), (1, XM, TM), (1, XP, TP), (0, XM, TM)):
        copy(xblock(w, x, crow), xblock(w, x, crow), to, base + w).start()
    for w in range(2):
        copy(xblock(w, x, crow), xblock(w, x, crow), PA, TC + w * 4).start()

    def ysend(slot, w, j):
        piece = wpiece(slot, w, y, j)
        copy(piece, piece, YPd, YP + slot * 8 + w * 4 + j).start()
        copy(piece, piece, YMd, YM + slot * 8 + w * 4 + j).start()

    @pl.when(p == 0)
    def _():
        for w in range(2):
            W[0, w, wrow(y, x), :] = WS[w]
            ysend(0, w, x)

    def root_forward():
        got(wpiece(0, 0, ym, x), YP + x)
        copy(wpiece(0, 0, ym, x), wpiece(0, 0, ym, x), YPd, YF + x).start()
        got(wpiece(0, 1, yp, x), YM + 4 + x)
        copy(wpiece(0, 1, yp, x), wpiece(0, 1, yp, x), YMd, YF + 4 + x).start()

    def root_rest():
        got(wpiece(0, 0, yp, x), YM + x)
        got(wpiece(0, 1, ym, x), YP + 4 + x)
        for w in range(2):
            got(wpiece(0, w, yo, x), YF + w * 4 + x)

    def place(m):
        w, i = m % 2, m // 2
        return w, jnp.where(m < 6, y, (y + i + 1) % 4), jnp.where(m < 6, (x + i + 1) % 4, x)

    def step_a(m):
        w, yy, j = place(m)
        piece = wpiece(0, w, yy, j)

        @pl.when((p == 0) & (m < 6))
        def _():
            got(piece, SX + w * 4 + j)

        @pl.when(p != 0)
        def _():
            got(piece, ZP + m)

        copy(piece, wpiece(jnp.where(p == 3, 1, 0), w, yy, j), ZPd, ZP + m).start()

        @pl.when(p == 0)
        def _():
            copy(piece, wpiece(1, w, yy, j), ZMd, ZM + m).start()

        @pl.when(m < 6)
        def _():
            ysend(0, w, j)

    def step_b(m):
        w, yy, j = place(m)
        piece = wpiece(1, w, yy, j)

        @pl.when(p == 0)
        def _():
            got(piece, ZP + m)

        @pl.when(p != 0)
        def _():
            got(piece, ZM + m)

        @pl.when(p >= 2)
        def _():
            copy(piece, piece, ZMd, ZM + m).start()

        @pl.when(m < 6)
        def _():
            ysend(1, w, j)

    def yforward(slot, m):
        w, j = m % 2, (x + m // 2 + 1) % 4

        @pl.when(w == 0)
        def _():
            piece = wpiece(slot, 0, ym, j)
            got(piece, YP + slot * 8 + j)
            copy(piece, piece, YPd, YF + slot * 8 + j).start()

        @pl.when(w == 1)
        def _():
            piece = wpiece(slot, 1, yp, j)
            got(piece, YM + slot * 8 + 4 + j)
            copy(piece, piece, YMd, YF + slot * 8 + 4 + j).start()

    def pass_on(w, r):
        xx = (x + r) % 4
        copy(xblock(w, xx, crow), xblock(w, xx, crow), PA, TC + w * 4 + r).start()

    near = jnp.where(p < 2, 0, 1)
    far = 1 - near
    root = p == 0
    lag_a = jnp.where(p == 3, 5, 0)
    lag_b = jnp.where(root, 20, jnp.where(p == 1, 5, 0))
    lag_far = jnp.where(root, 28, jnp.where(p == 2, 8, 13))

    def zstep(t):
        @pl.when(root & (t == 2))
        def _():
            root_forward()

        @pl.when(root & (t == 6))
        def _():
            root_rest()

        @pl.when((t >= lag_a) & (t < lag_a + 14))
        def _():
            step_a(t - lag_a)

        @pl.when((t >= lag_b) & (t < lag_b + 14))
        def _():
            step_b(t - lag_b)

        @pl.when(t == jnp.where(root, 14, 6))
        def _():
            got(xblock(0, xm, crow), TP)
            copy(xblock(0, xm, crow), xblock(0, xm, crow), XP, TF).start()
            got(xblock(1, xp, crow), TM + 1)
            copy(xblock(1, xp, crow), xblock(1, xp, crow), XM, TF + 1).start()
            pass_on(0, 3)
            pass_on(1, 1)

        @pl.when(root & (t >= 14) & (t < 20))
        def _():
            yforward(near, t - 14)

        @pl.when((p != 0) & (t >= 4) & (t < 16) & (t % 2 == 0))
        def _():
            yforward(near, (t - 4) // 2)

        @pl.when((t >= lag_far) & (t < lag_far + 6))
        def _():
            yforward(far, t - lag_far)

        @pl.when(t == jnp.where(root, 26, 13))
        def _():
            got(xblock(1, xm, crow), TP + 1)
            pass_on(1, 3)
            got(xblock(0, xp, crow), TM)
            pass_on(0, 1)

    both(34, zstep)

    def yfinish(slot):
        def piece(i):
            j = (x + i + 1) % 4
            got(wpiece(slot, 0, yp, j), YM + slot * 8 + j)
            got(wpiece(slot, 1, ym, j), YP + slot * 8 + 4 + j)
            for w in range(2):
                got(wpiece(slot, w, yo, j), YF + slot * 8 + w * 4 + j)

        both(3, piece)

    orow = pl.ds(pl.multiple_of((1 - c) * 128, 128), 128)

    def partner(r):
        for w in range(2):
            got(xblock(w, (x + r) % 4, orow), TC + w * 4 + r)

    def act(slot, r):
        xx = (x + r) % 4
        pre = jnp.dot(X[0, xx], W[slot, 0], preferred_element_type=F32)
        dh = jnp.dot(X[1, xx], W[slot, 1], preferred_element_type=F32)
        active = jnp.maximum(pre, 0.0)
        hidden = active * active
        dpre = 2.0 * active * dh
        DP[slot, pl.ds(pl.multiple_of(xx * 256, 256), 256), :] = dpre.astype(BF)
        cols = pl.ds(pl.multiple_of(xx * 256, 256), 256)
        TT[slot, 0, :, cols] = dpre.T.astype(BF)
        TT[slot, 1, :, cols] = hidden.T.astype(BF)

    def act_three(slot):
        both(3, lambda i: act(slot, jnp.where(i == 2, 3, i)))

    yfinish(near)
    partner(0)
    partner(1)
    partner(3)
    act_three(near)
    got(xblock(0, xo, crow), TF)
    pass_on(0, 2)
    got(xblock(1, xo, crow), TF + 1)
    pass_on(1, 2)
    yfinish(far)
    act_three(far)
    partner(2)

    def grads(slot, send):
        def block(i):
            yy = (y + jnp.where(i < 2, 2 - i, i + 1)) % 4
            cols = pl.ds(pl.multiple_of(yy * 512, 512), 512)
            for w in range(2):
                rows = X[w, :, :, cols].reshape(1024, 512)
                part = jnp.dot(TT[slot, w], rows, preferred_element_type=F32).astype(BF)
                for j in range(4):
                    G[slot, w, yy, (j - x + 4) % 4] = part[:, j * 128 : (j + 1) * 128]
            if send:
                for at in range(3):

                    @pl.when(i == at)
                    def _(at=at):
                        ab(slot, at)

        both(4, block)

    rest = pl.ds(1, 3)

    def ab(slot, at):
        base = GY + slot * 4
        if at == 0:
            copy(G.at[slot, 0, yo, rest], RY.at[slot, 0, 0], YPd, base).start()
            copy(G.at[slot, 1, yo, rest], RY.at[slot, 1, 0], YMd, base + 1).start()
        if at == 1:
            copy(G.at[slot, 1, yp, rest], RY.at[slot, 0, 1], YPd, base + 2).start()
        if at == 2:
            copy(G.at[slot, 0, ym, rest], RY.at[slot, 1, 1], YMd, base + 3).start()

    def add(*terms):
        total = terms[0].astype(F32)
        for term in terms[1:]:
            total = total + term.astype(F32)
        return total.astype(BF)

    def cstep(slot):
        base = GY + slot * 4
        got(RY.at[slot, 0, 0], base)
        got(RY.at[slot, 1, 0], base + 1)

        def piece(i):
            G[slot, 0, yp, i + 1] = add(G[slot, 0, yp, i + 1], RY[slot, 0, 0, i])
            copy(G.at[slot, 0, yp, i + 1], RC.at[slot, 0, i], YPd, GC + slot * 6 + i).start()
            G[slot, 1, ym, i + 1] = add(G[slot, 1, ym, i + 1], RY[slot, 1, 0, i])
            copy(G.at[slot, 1, ym, i + 1], RC.at[slot, 1, i], YMd, GC + slot * 6 + 3 + i).start()

        both(3, piece)

    def chain_b(m):
        w, i = m % 2, m // 2 + 1

        @pl.when(root)
        def _():
            copy(G.at[1, w, y, i], ZA.at[m], ZMd, GA + m).start()

        @pl.when(p >= 2)
        def _():
            got(ZB.at[m], GB + m)
            G[1, w, y, i] = add(G[1, w, y, i], ZB[m])

        @pl.when(p != 0)
        def _():
            copy(G.at[1, w, y, i], ZB.at[m], ZPd, GB + m).start()

    def chain_a(m):
        w, i = m % 2, m // 2 + 1
        got(ZA.at[m], GA + m)

        @pl.when(p != 0)
        def _():
            G[0, w, y, i] = add(G[0, w, y, i], ZA[m])
            copy(G.at[0, w, y, i], ZA.at[m], ZMd, GA + m).start()

        @pl.when(root)
        def _():
            got(ZB.at[m], GB + m)
            G[0, w, y, i] = add(G[0, w, y, i], ZA[m], ZB[m])
            copy(G.at[0, w, y, i], FX.at[w], dev(y, (x + i) % 4, z, c), FS + w, FSS + w * 4 + i).start()

    def yfinal(slot, after):
        base = GY + slot * 4
        got(RY.at[slot, 0, 1], base + 2)
        got(RY.at[slot, 1, 1], base + 3)

        def piece(i):
            got(RC.at[slot, 0, i], GC + slot * 6 + i)
            G[slot, 0, y, i + 1] = add(G[slot, 0, y, i + 1], RC[slot, 0, i], RY[slot, 1, 1, i])
            got(RC.at[slot, 1, i], GC + slot * 6 + 3 + i)
            G[slot, 1, y, i + 1] = add(G[slot, 1, y, i + 1], RC[slot, 1, i], RY[slot, 0, 1, i])
            after(i)

        both(3, piece)

    def qplace(q):
        i = q // 2
        return q % 2, (y + jnp.where(i < 2, 2 - i, i + 1)) % 4

    def own_b(q):
        w, yy = qplace(q)

        @pl.when(root)
        def _():
            copy(G.at[1, w, yy, 0], UA.at[q], ZMd, QA + q).start()

        @pl.when(p >= 2)
        def _():
            got(UB.at[q], QB + q)
            G[1, w, yy, 0] = add(G[1, w, yy, 0], UB[q])

        @pl.when(p != 0)
        def _():
            copy(G.at[1, w, yy, 0], UB.at[q], ZPd, QB + q).start()

    def own_a(q):
        w, yy = qplace(q)
        got(UA.at[q], QA + q)

        @pl.when(p != 0)
        def _():
            G[0, w, yy, 0] = add(G[0, w, yy, 0], UA[q])
            copy(G.at[0, w, yy, 0], UA.at[q], ZMd, QA + q).start()

        @pl.when(root)
        def _():
            got(UB.at[q], QB + q)
            G[0, w, yy, 0] = add(G[0, w, yy, 0], UA[q], UB[q])

            @pl.when(q == 0)
            def _():
                copy(G.at[0, 0, yo, 0], RG.at[0, 0], YPd, RS).start()

            @pl.when(q == 1)
            def _():
                copy(G.at[0, 1, yo, 0], RG.at[1, 0], YMd, RS + 1).start()

            @pl.when(q == 3)
            def _():
                copy(G.at[0, 1, yp, 0], RG.at[0, 1], YPd, RS + 2).start()

            @pl.when(q == 4)
            def _():
                copy(G.at[0, 0, ym, 0], RG.at[1, 1], YMd, RS + 3).start()

    def igrad(n):
        rows = pl.ds(pl.multiple_of(n * 256, 256), 256)
        nt = (((1,), (1,)), ((), ()))
        part = lax.dot_general(DP[0], W[0, 0, rows, :], nt, preferred_element_type=F32)
        part = part + lax.dot_general(DP[1], W[1, 0, rows, :], nt, preferred_element_type=F32)
        part = part.astype(BF).reshape(4, 2, 128, 256)
        cols = pl.ds(pl.multiple_of((n % 4) * 256, 256), 256)
        for cc in range(2):
            S[cc, n // 4, :, :, cols] = part[:, cc]

    act(far, 2)
    grads(far, True)

    @pl.when(p < 2)
    def _():
        both(8, own_b)

    act(near, 2)
    grads(near, False)
    cstep(far)
    for at in range(3):
        ab(near, at)
    for half in range(2):
        both(4, lambda n, half=half: igrad(half * 4 + n))
        copy(S.at[1 - c, half], RP.at[half], PA, XC + half).start()

    for half in range(2):
        got(RP.at[half], XC + half)

        def xadd(r, half=half):
            S[c, half, r] = add(S[c, half, r], RP[half, r])

        both(4, xadd)
    copy(S.at[c, 0, xo], XR.at[0, 0], XP, XY).start()
    copy(S.at[c, 1, xo], XR.at[1, 0], XM, XY + 1).start()
    copy(S.at[c, 1, xp], XR.at[0, 1], XP, XY + 2).start()
    copy(S.at[c, 0, xm], XR.at[1, 1], XM, XY + 3).start()

    @pl.when(p >= 2)
    def _():
        both(8, own_a)

    def head(i):
        @pl.when(p < 2)
        def _():
            chain_b(i * 2)
            chain_b(i * 2 + 1)

    yfinal(far, head)
    cstep(near)

    @pl.when(p == 1)
    def _():
        both(8, own_a)

    @pl.when(p == 2)
    def _():
        both(8, own_b)

    @pl.when(p >= 2)
    def _():
        both(6, chain_a)

    @pl.when(p == 3)
    def _():
        both(8, own_b)

    got(XR.at[0, 0], XY)
    S[c, 0, xp] = add(S[c, 0, xp], XR[0, 0])
    copy(S.at[c, 0, xp], XR.at[0, 2], XP, XY + 4).start()
    got(XR.at[1, 0], XY + 1)
    S[c, 1, xm] = add(S[c, 1, xm], XR[1, 0])
    copy(S.at[c, 1, xm], XR.at[1, 2], XM, XY + 5).start()

    def tail(i):
        @pl.when(p == 1)
        def _():
            chain_a(i * 2)
            chain_a(i * 2 + 1)

        @pl.when(p >= 2)
        def _():
            chain_b(i * 2)
            chain_b(i * 2 + 1)

    yfinal(near, tail)

    @pl.when(root)
    def _():
        both(8, own_a)
        both(6, chain_a)
        got(RG.at[0, 0], RS)
        G[0, 0, yp, 0] = add(G[0, 0, yp, 0], RG[0, 0])
        copy(G.at[0, 0, yp, 0], RG.at[0, 2], YPd, RS + 4).start()
        got(RG.at[1, 0], RS + 1)
        G[0, 1, ym, 0] = add(G[0, 1, ym, 0], RG[1, 0])
        copy(G.at[0, 1, ym, 0], RG.at[1, 2], YMd, RS + 5).start()

    got(XR.at[0, 1], XY + 2)
    got(XR.at[1, 1], XY + 3)
    got(XR.at[0, 2], XY + 4)
    got(XR.at[1, 2], XY + 5)
    for half, (d0, k0), (d1, k1) in ((0, (0, 2), (1, 1)), (1, (0, 1), (1, 2))):
        ig_out[:, half * 1024 : (half + 1) * 1024] = add(S[c, half, x], XR[d0, k0], XR[d1, k1])

    @pl.when(root)
    def _():
        for k in range(1, 5):
            got(RG.at[(k + 1) % 2, (k + 1) // 2], RS + k + 1)
        FX[0] = add(G[0, 0, y, 0], RG[0, 2], RG[1, 1])
        FX[1] = add(G[0, 1, y, 0], RG[0, 1], RG[1, 2])

    @pl.when(p != 0)
    def _():
        for w in range(2):
            got(FX.at[w], FS + w)

    ug_out[...] = FX[0].astype(F32).T * factor
    dg_out[...] = FX[1].astype(F32) * factor

    unit = FX.at[0]

    @pl.when(p != 0)
    def _():
        for w in range(2):
            sent(unit, SX + w * 4 + x)

    def chain_sends(m):
        sent(unit, ZP + m)

        @pl.when(p != 1)
        def _():
            sent(unit, ZM + m)

    both(14, chain_sends)

    def sends(k):
        w, j = k // 4, k % 4
        for slot in range(2):

            @pl.when((j != x) | (root & (slot == 0)))
            def _(slot=slot):
                for base in (YP, YM, YF):
                    sent(unit, base + slot * 8 + k)

        sent(UA.at[k], QA + k)

        @pl.when(p != 0)
        def _():
            sent(UB.at[k], QB + k)

        @pl.when(root & (j != 0))
        def _():
            sent(unit, FSS + k)

        sent(xblock(w, x, crow), TC + k)
        sent(RY.at[0, 0, 0], GY + k)

    both(8, sends)

    def more_sends(m):
        sent(unit, GC + m)
        sent(unit, GC + 6 + m)
        sent(unit, GA + m)

        @pl.when(p != 0)
        def _():
            sent(unit, GB + m)

        @pl.when(root)
        def _():
            sent(unit, RS + m)

        sent(xblock(0, x, crow), TP + m)
        sent(XR.at[0, 0], XY + m)

    both(6, more_sends)
    for i in range(2):
        sent(RP.at[0], XC + i)


def solution(mesh):
    def shards(tokens, up_weight, down_weight, cotangent):
        count_all = tokens.shape[0] * lax.axis_size("fs") * lax.axis_size("tp")
        factor = 1.0 / float(count_all) ** 0.5
        vmem = pl.BlockSpec(memory_space=pltpu.VMEM)
        hbm = pl.BlockSpec(memory_space=pl.ANY)

        def body(*refs):
            kernel(factor, *refs)

        return pl.pallas_call(
            body,
            out_shape=(
                jax.ShapeDtypeStruct((128, 2048), BF),
                jax.ShapeDtypeStruct((128, 256), F32),
                jax.ShapeDtypeStruct((256, 128), F32),
            ),
            in_specs=[hbm, vmem, vmem, hbm],
            out_specs=(vmem, vmem, vmem),
            scratch_shapes=[
                pltpu.VMEM((2, 4, 256, 2048), BF),
                pltpu.VMEM((2, 128, 256), BF),
                pltpu.VMEM((2, 2, 2048, 256), BF),
                pltpu.VMEM((2, 1024, 256), BF),
                pltpu.VMEM((2, 2, 256, 1024), BF),
                pltpu.VMEM((2, 2, 4, 4, 256, 128), BF),
                pltpu.VMEM((2, 2, 2, 3, 256, 128), BF),
                pltpu.VMEM((2, 2, 3, 256, 128), BF),
                pltpu.VMEM((6, 256, 128), BF),
                pltpu.VMEM((6, 256, 128), BF),
                pltpu.VMEM((8, 256, 128), BF),
                pltpu.VMEM((8, 256, 128), BF),
                pltpu.VMEM((2, 3, 256, 128), BF),
                pltpu.VMEM((2, 256, 128), BF),
                pltpu.VMEM((2, 2, 4, 128, 1024), BF),
                pltpu.VMEM((2, 4, 128, 1024), BF),
                pltpu.VMEM((2, 3, 128, 1024), BF),
                pltpu.SemaphoreType.DMA((N_SEM,)),
                pltpu.SemaphoreType.DMA((N_SEM,)),
                pltpu.SemaphoreType.DMA((2,)),
            ],
            compiler_params=pltpu.CompilerParams(
                collective_id=0, has_side_effects=True, vmem_limit_bytes=60 * 2**20
            ),
            name="ffn_backward",
        )(tokens, up_weight, down_weight, cotangent)

    placed = (P(("fs", "tp"), None), P("fs", "tp"), P("tp", "fs"), P(("fs", "tp"), None))
    return jax.shard_map(
        shards,
        mesh=mesh,
        in_specs=placed,
        out_specs=(P(("fs", "tp"), None), P("fs", "tp"), P("tp", "fs")),
        check_vma=False,
    )
```

time: 128 us -> 117 us (0.914)
  the two profiles are of different devices: /device:TPU:4 before, /device:TPU:35 now
where the time goes in v2:
time: 117 us
  Pallas kernels  113 us (97%)
  local copies, waits for them, and re-layouts  3.53 us (3%)
    pallas_call x1, Pallas kernels, shards(): pl.pallas_call(body, out_shape=(jax.ShapeDtypeStruct((128, 2048), BF), ja...  113 us
    unnamed x7, local copies, waits for them, and re-layouts  3.53 us

profile of v2, /device:TPU:35, one launch (start us, length us, event | category | flops | bytes accessed | tf_op | source)
XLA Modules:
  0.0 116.8 jit_solution(8050757727623759325)
XLA Ops:
  0.6 112.7 %ffn_backward.1 = (bf16[128,2048]{1,0:T(8,128)(2,1)}, f32[128,256]{1,0:T(8,128)}, f32[256,128]{1,0:T(8,128)}) custom-call(bf16[128,2048]{1,0:T(8,128)(2,1)} %refs_0_.1, bf16[128,256]{1,0:T(8,128)(2,1)} %refs_1_.1, bf16[256,128]{1,0:T(8,128)(2,1)} %refs_2_.1, bf16[128,2048]{1,0:T(8,128)(2,1)} %refs_3_.1), custom_call_target="tpu_custom_call" | custom-call | tf_op jit(solution)/shard_map/ffn_backward/pallas_call | solution.py:615
  113.3 0.0 copy-start.1
  113.3 1.9 %copy.10 = bf16[128,2048]{1,0:T(8,128)(2,1)} copy(bf16[128,2048]{1,0:T(8,128)(2,1)} %get-tuple-element.6) | data formatting | bytes 1048576
  115.2 0.0 copy-done.1
  115.2 0.0 copy-start
  115.2 0.7 copy.11
  115.9 0.3 copy-done
  116.2 0.7 copy.12
Async XLA Ops:
  113.3 1.9 %copy-start.1 = (f32[128,256]{1,0:T(8,128)S(1)}, f32[128,256]{1,0:T(8,128)}, u32[]{:S(2)}) copy-start(f32[128,256]{1,0:T(8,128)} %get-tuple-element.7) | copy-start | bytes 393220
  115.2 1.0 copy-start

commit v3 on v2

--- a/solution.py
+++ b/solution.py
@@ -11,9 +11,9 @@
 
 SX, ZP, ZM, YP, YM, YF = 0, 8, 22, 36, 52, 68
 TP, TM, TF, TC = 84, 86, 88, 90
-GY, GC, GA, GB, QA, QB, RS = 98, 106, 118, 124, 130, 138, 146
-FS, FSS, XC, XY = 152, 154, 162, 164
-N_SEM = 170
+AY, BY, GC, GA, GB, QA, QB, RS = 98, 110, 122, 134, 140, 146, 154, 162
+FS, FSS, XC, XY = 168, 170, 178, 180
+N_SEM = 186
 
 
 def both(n, body):
@@ -186,53 +186,6 @@
     lag_b = jnp.where(root, 20, jnp.where(p == 1, 5, 0))
     lag_far = jnp.where(root, 28, jnp.where(p == 2, 8, 13))
 
-    def zstep(t):
-        @pl.when(root & (t == 2))
-        def _():
-            root_forward()
-
-        @pl.when(root & (t == 6))
-        def _():
-            root_rest()
-
-        @pl.when((t >= lag_a) & (t < lag_a + 14))
-        def _():
-            step_a(t - lag_a)
-
-        @pl.when((t >= lag_b) & (t < lag_b + 14))
-        def _():
-            step_b(t - lag_b)
-
-        @pl.when(t == jnp.where(root, 14, 6))
-        def _():
-            got(xblock(0, xm, crow), TP)
-            copy(xblock(0, xm, crow), xblock(0, xm, crow), XP, TF).start()
-            got(xblock(1, xp, crow), TM + 1)
-            copy(xblock(1, xp, crow), xblock(1, xp, crow), XM, TF + 1).start()
-            pass_on(0, 3)
-            pass_on(1, 1)
-
-        @pl.when(root & (t >= 14) & (t < 20))
-        def _():
-            yforward(near, t - 14)
-
-        @pl.when((p != 0) & (t >= 4) & (t < 16) & (t % 2 == 0))
-        def _():
-            yforward(near, (t - 4) // 2)
-
-        @pl.when((t >= lag_far) & (t < lag_far + 6))
-        def _():
-            yforward(far, t - lag_far)
-
-        @pl.when(t == jnp.where(root, 26, 13))
-        def _():
-            got(xblock(1, xm, crow), TP + 1)
-            pass_on(1, 3)
-            got(xblock(0, xp, crow), TM)
-            pass_on(0, 1)
-
-    both(34, zstep)
-
     def yfinish(slot):
         def piece(i):
             j = (x + i + 1) % 4
@@ -264,11 +217,65 @@
     def act_three(slot):
         both(3, lambda i: act(slot, jnp.where(i == 2, 3, i)))
 
-    yfinish(near)
-    partner(0)
-    partner(1)
-    partner(3)
-    act_three(near)
+    def near_part():
+        yfinish(near)
+        partner(0)
+        partner(1)
+        partner(3)
+        act_three(near)
+
+    def zstep(t):
+        @pl.when(root & (t == 2))
+        def _():
+            root_forward()
+
+        @pl.when(root & (t == 6))
+        def _():
+            root_rest()
+
+        @pl.when((t >= lag_a) & (t < lag_a + 14))
+        def _():
+            step_a(t - lag_a)
+
+        @pl.when((t >= lag_b) & (t < lag_b + 14))
+        def _():
+            step_b(t - lag_b)
+
+        @pl.when(t == jnp.where(root, 14, 6))
+        def _():
+            got(xblock(0, xm, crow), TP)
+            copy(xblock(0, xm, crow), xblock(0, xm, crow), XP, TF).start()
+            got(xblock(1, xp, crow), TM + 1)
+            copy(xblock(1, xp, crow), xblock(1, xp, crow), XM, TF + 1).start()
+            pass_on(0, 3)
+            pass_on(1, 1)
+
+        @pl.when(root & (t >= 14) & (t < 20))
+        def _():
+            yforward(near, t - 14)
+
+        @pl.when((p != 0) & (t >= 4) & (t < 16) & (t % 2 == 0))
+        def _():
+            yforward(near, (t - 4) // 2)
+
+        @pl.when((t >= lag_far) & (t < lag_far + 6))
+        def _():
+            yforward(far, t - lag_far)
+
+        @pl.when(t == jnp.where(root, 26, 13))
+        def _():
+            got(xblock(1, xm, crow), TP + 1)
+            pass_on(1, 3)
+            got(xblock(0, xp, crow), TM)
+            pass_on(0, 1)
+
+        @pl.when(root & (t == 27))
+        def _():
+            near_part()
+
+    both(34, zstep)
+
+    pl.when(p != 0)(near_part)
     got(xblock(0, xo, crow), TF)
     pass_on(0, 2)
     got(xblock(1, xo, crow), TF + 1)
@@ -287,25 +294,28 @@
                 for j in range(4):
                     G[slot, w, yy, (j - x + 4) % 4] = part[:, j * 128 : (j + 1) * 128]
             if send:
-                for at in range(3):
+                for at, copies in enumerate((a_send, bp_send, bm_send)):
 
                     @pl.when(i == at)
-                    def _(at=at):
-                        ab(slot, at)
+                    def _(copies=copies):
+                        both(3, lambda n: copies(slot, n))
 
         both(4, block)
 
-    rest = pl.ds(1, 3)
-
-    def ab(slot, at):
-        base = GY + slot * 4
-        if at == 0:
-            copy(G.at[slot, 0, yo, rest], RY.at[slot, 0, 0], YPd, base).start()
-            copy(G.at[slot, 1, yo, rest], RY.at[slot, 1, 0], YMd, base + 1).start()
-        if at == 1:
-            copy(G.at[slot, 1, yp, rest], RY.at[slot, 0, 1], YPd, base + 2).start()
-        if at == 2:
-            copy(G.at[slot, 0, ym, rest], RY.at[slot, 1, 1], YMd, base + 3).start()
+    def a_send(slot, i):
+        copy(G.at[slot, 0, yo, i + 1], RY.at[slot, 0, 0, i], YPd, AY + slot * 6 + i).start()
+        copy(G.at[slot, 1, yo, i + 1], RY.at[slot, 1, 0, i], YMd, AY + slot * 6 + 3 + i).start()
+
+    def bp_send(slot, i):
+        copy(G.at[slot, 1, yp, i + 1], RY.at[slot, 0, 1, i], YPd, BY + slot * 6 + i).start()
+
+    def bm_send(slot, i):
+        copy(G.at[slot, 0, ym, i + 1], RY.at[slot, 1, 1, i], YMd, BY + slot * 6 + 3 + i).start()
+
+    def ab_send(slot, i):
+        a_send(slot, i)
+        bp_send(slot, i)
+        bm_send(slot, i)
 
     def add(*terms):
         total = terms[0].astype(F32)
@@ -313,18 +323,13 @@
             total = total + term.astype(F32)
         return total.astype(BF)
 
-    def cstep(slot):
-        base = GY + slot * 4
-        got(RY.at[slot, 0, 0], base)
-        got(RY.at[slot, 1, 0], base + 1)
-
-        def piece(i):
-            G[slot, 0, yp, i + 1] = add(G[slot, 0, yp, i + 1], RY[slot, 0, 0, i])
-            copy(G.at[slot, 0, yp, i + 1], RC.at[slot, 0, i], YPd, GC + slot * 6 + i).start()
-            G[slot, 1, ym, i + 1] = add(G[slot, 1, ym, i + 1], RY[slot, 1, 0, i])
-            copy(G.at[slot, 1, ym, i + 1], RC.at[slot, 1, i], YMd, GC + slot * 6 + 3 + i).start()
-
-        both(3, piece)
+    def c_step(slot, i):
+        got(RY.at[slot, 0, 0, i], AY + slot * 6 + i)
+        G[slot, 0, yp, i + 1] = add(G[slot, 0, yp, i + 1], RY[slot, 0, 0, i])
+        copy(G.at[slot, 0, yp, i + 1], RC.at[slot, 0, i], YPd, GC + slot * 6 + i).start()
+        got(RY.at[slot, 1, 0, i], AY + slot * 6 + 3 + i)
+        G[slot, 1, ym, i + 1] = add(G[slot, 1, ym, i + 1], RY[slot, 1, 0, i])
+        copy(G.at[slot, 1, ym, i + 1], RC.at[slot, 1, i], YMd, GC + slot * 6 + 3 + i).start()
 
     def chain_b(m):
         w, i = m % 2, m // 2 + 1
@@ -357,19 +362,13 @@
             G[0, w, y, i] = add(G[0, w, y, i], ZA[m], ZB[m])
             copy(G.at[0, w, y, i], FX.at[w], dev(y, (x + i) % 4, z, c), FS + w, FSS + w * 4 + i).start()
 
-    def yfinal(slot, after):
-        base = GY + slot * 4
-        got(RY.at[slot, 0, 1], base + 2)
-        got(RY.at[slot, 1, 1], base + 3)
-
-        def piece(i):
-            got(RC.at[slot, 0, i], GC + slot * 6 + i)
-            G[slot, 0, y, i + 1] = add(G[slot, 0, y, i + 1], RC[slot, 0, i], RY[slot, 1, 1, i])
-            got(RC.at[slot, 1, i], GC + slot * 6 + 3 + i)
-            G[slot, 1, y, i + 1] = add(G[slot, 1, y, i + 1], RC[slot, 1, i], RY[slot, 0, 1, i])
-            after(i)
-
-        both(3, piece)
+    def y_final(slot, i):
+        got(RY.at[slot, 1, 1, i], BY + slot * 6 + 3 + i)
+        got(RC.at[slot, 0, i], GC + slot * 6 + i)
+        G[slot, 0, y, i + 1] = add(G[slot, 0, y, i + 1], RC[slot, 0, i], RY[slot, 1, 1, i])
+        got(RY.at[slot, 0, 1, i], BY + slot * 6 + i)
+        got(RC.at[slot, 1, i], GC + slot * 6 + 3 + i)
+        G[slot, 1, y, i + 1] = add(G[slot, 1, y, i + 1], RC[slot, 1, i], RY[slot, 0, 1, i])
 
     def qplace(q):
         i = q // 2
@@ -440,78 +439,31 @@
 
     act(near, 2)
     grads(near, False)
-    cstep(far)
-    for at in range(3):
-        ab(near, at)
-    for half in range(2):
-        both(4, lambda n, half=half: igrad(half * 4 + n))
-        copy(S.at[1 - c, half], RP.at[half], PA, XC + half).start()
-
-    for half in range(2):
+    both(3, lambda i: c_step(far, i))
+    both(2, lambda i: ab_send(near, i))
+
+    def x_first(half):
         got(RP.at[half], XC + half)
-
-        def xadd(r, half=half):
-            S[c, half, r] = add(S[c, half, r], RP[half, r])
-
-        both(4, xadd)
-    copy(S.at[c, 0, xo], XR.at[0, 0], XP, XY).start()
-    copy(S.at[c, 1, xo], XR.at[1, 0], XM, XY + 1).start()
-    copy(S.at[c, 1, xp], XR.at[0, 1], XP, XY + 2).start()
-    copy(S.at[c, 0, xm], XR.at[1, 1], XM, XY + 3).start()
-
-    @pl.when(p >= 2)
-    def _():
-        both(8, own_a)
-
-    def head(i):
-        @pl.when(p < 2)
-        def _():
-            chain_b(i * 2)
-            chain_b(i * 2 + 1)
-
-    yfinal(far, head)
-    cstep(near)
-
-    @pl.when(p == 1)
-    def _():
-        both(8, own_a)
-
-    @pl.when(p == 2)
-    def _():
-        both(8, own_b)
-
-    @pl.when(p >= 2)
-    def _():
-        both(6, chain_a)
-
-    @pl.when(p == 3)
-    def _():
-        both(8, own_b)
-
-    got(XR.at[0, 0], XY)
-    S[c, 0, xp] = add(S[c, 0, xp], XR[0, 0])
-    copy(S.at[c, 0, xp], XR.at[0, 2], XP, XY + 4).start()
-    got(XR.at[1, 0], XY + 1)
-    S[c, 1, xm] = add(S[c, 1, xm], XR[1, 0])
-    copy(S.at[c, 1, xm], XR.at[1, 2], XM, XY + 5).start()
-
-    def tail(i):
-        @pl.when(p == 1)
-        def _():
-            chain_a(i * 2)
-            chain_a(i * 2 + 1)
-
-        @pl.when(p >= 2)
-        def _():
-            chain_b(i * 2)
-            chain_b(i * 2 + 1)
-
-    yfinal(near, tail)
-
-    @pl.when(root)
-    def _():
-        both(8, own_a)
-        both(6, chain_a)
+        both(4, lambda r: xadd(half, r))
+
+    def xadd(half, r):
+        S[c, half, r] = add(S[c, half, r], RP[half, r])
+
+    def x_send():
+        copy(S.at[c, 0, xo], XR.at[0, 0], XP, XY).start()
+        copy(S.at[c, 1, xo], XR.at[1, 0], XM, XY + 1).start()
+        copy(S.at[c, 1, xp], XR.at[0, 1], XP, XY + 2).start()
+        copy(S.at[c, 0, xm], XR.at[1, 1], XM, XY + 3).start()
+
+    def x_second():
+        got(XR.at[0, 0], XY)
+        S[c, 0, xp] = add(S[c, 0, xp], XR[0, 0])
+        copy(S.at[c, 0, xp], XR.at[0, 2], XP, XY + 4).start()
+        got(XR.at[1, 0], XY + 1)
+        S[c, 1, xm] = add(S[c, 1, xm], XR[1, 0])
+        copy(S.at[c, 1, xm], XR.at[1, 2], XM, XY + 5).start()
+
+    def root_second():
         got(RG.at[0, 0], RS)
         G[0, 0, yp, 0] = add(G[0, 0, yp, 0], RG[0, 0])
         copy(G.at[0, 0, yp, 0], RG.at[0, 2], YPd, RS + 4).start()
@@ -519,6 +471,87 @@
         G[0, 1, ym, 0] = add(G[0, 1, ym, 0], RG[1, 0])
         copy(G.at[0, 1, ym, 0], RG.at[1, 2], YMd, RS + 5).start()
 
+    def by_p(*values):
+        return jnp.where(p == 0, values[0], jnp.where(p == 1, values[1], jnp.where(p == 2, values[2], values[3])))
+
+    never = 99
+    at_own_b = by_p(never, never, 1, 3)
+    at_own_a = by_p(12, 9, 6, 3)
+    at_chain_a = by_p(20, 18, 13, 10)
+    at_chain_b = by_p(never, never, never, 18)
+
+    def rstep(t):
+        def span(start, count, body):
+            @pl.when((t >= start) & (t < start + count))
+            def _():
+                body(t - start)
+
+        span(at_own_b, 8, own_b)
+        span(at_own_a, 8, own_a)
+        span(at_chain_b, 6, chain_b)
+
+        @pl.when(root & (t == 20))
+        def _():
+            root_second()
+
+        span(at_chain_a, 6, chain_a)
+
+        @pl.when(t < 4)
+        def _():
+            igrad(t * 2)
+            igrad(t * 2 + 1)
+
+        @pl.when((t == 1) | (t == 3))
+        def _():
+            half = t // 2
+            copy(S.at[1 - c, half], RP.at[half], PA, XC + half).start()
+
+        @pl.when((t == 5) | (t == 6))
+        def _():
+            x_first(t - 5)
+
+        @pl.when(t == 6)
+        def _():
+            x_send()
+
+        @pl.when(t == 8)
+        def _():
+            def piece(i):
+                y_final(far, i)
+
+                @pl.when(p < 2)
+                def _():
+                    chain_b(i * 2)
+                    chain_b(i * 2 + 1)
+
+            both(3, piece)
+
+        span(9, 2, lambda i: c_step(near, i))
+
+        @pl.when(t == 10)
+        def _():
+            ab_send(near, 2)
+
+        @pl.when(t == 12)
+        def _():
+            x_second()
+
+        @pl.when(t == 14)
+        def _():
+            c_step(near, 2)
+
+        @pl.when((t == 13) | (t == 15) | (t == 17))
+        def _():
+            i = (t - 13) // 2
+            y_final(near, i)
+
+            @pl.when(p == 2)
+            def _():
+                chain_b(i * 2)
+                chain_b(i * 2 + 1)
+
+    both(26, rstep)
+
     got(XR.at[0, 1], XY + 2)
     got(XR.at[1, 1], XY + 3)
     got(XR.at[0, 2], XY + 4)
@@ -577,13 +610,15 @@
             sent(unit, FSS + k)
 
         sent(xblock(w, x, crow), TC + k)
-        sent(RY.at[0, 0, 0], GY + k)
 
     both(8, sends)
 
     def more_sends(m):
         sent(unit, GC + m)
         sent(unit, GC + 6 + m)
+        for base in (AY, BY):
+            sent(unit, base + m)
+            sent(unit, base + 6 + m)
         sent(unit, GA + m)
 
         @pl.when(p != 0)

time: 117 us -> 108 us (0.923)
  the two profiles are of different devices: /device:TPU:35 before, /device:TPU:4 now
where the time goes in v3:
time: 108 us; the launch traced here: 105 us
  Pallas kernels  101 us (94%)
  local copies, waits for them, and re-layouts  3.53 us (3%)
    pallas_call x1, Pallas kernels, shards(): pl.pallas_call(body, out_shape=(jax.ShapeDtypeStruct((128, 2048), BF), ja...  101 us
    unnamed x7, local copies, waits for them, and re-layouts  3.53 us

profile of v3, /device:TPU:4, one launch (start us, length us, event | category | flops | bytes accessed | tf_op | source)
XLA Modules:
  0.0 105.5 jit_solution(8706194021410589296)
XLA Ops:
  0.6 101.3 %ffn_backward.1 = (bf16[128,2048]{1,0:T(8,128)(2,1)}, f32[128,256]{1,0:T(8,128)}, f32[256,128]{1,0:T(8,128)}) custom-call(bf16[128,2048]{1,0:T(8,128)(2,1)} %refs_0_.1, bf16[128,256]{1,0:T(8,128)(2,1)} %refs_1_.1, bf16[256,128]{1,0:T(8,128)(2,1)} %refs_2_.1, bf16[128,2048]{1,0:T(8,128)(2,1)} %refs_3_.1), custom_call_target="tpu_custom_call" | custom-call | tf_op jit(solution)/shard_map/ffn_backward/pallas_call | solution.py:650
  101.9 0.0 copy-start.1
  102.0 1.9 %copy.10 = bf16[128,2048]{1,0:T(8,128)(2,1)} copy(bf16[128,2048]{1,0:T(8,128)(2,1)} %get-tuple-element.6) | data formatting | bytes 1048576
  103.9 0.0 copy-done.1
  103.9 0.0 copy-start
  103.9 0.7 copy.11
  104.5 0.3 copy-done
  104.8 0.7 copy.12
Async XLA Ops:
  101.9 1.9 %copy-start.1 = (f32[128,256]{1,0:T(8,128)S(1)}, f32[128,256]{1,0:T(8,128)}, u32[]{:S(2)}) copy-start(f32[128,256]{1,0:T(8,128)} %get-tuple-element.7) | copy-start | bytes 393220
  103.9 1.0 copy-start

commit v4 on v3

--- a/solution.py
+++ b/solution.py
@@ -116,13 +116,13 @@
 
     def place(m):
         w, i = m % 2, m // 2
-        return w, jnp.where(m < 6, y, (y + i + 1) % 4), jnp.where(m < 6, (x + i + 1) % 4, x)
+        return w, jnp.where(i < 4, y, (y + i + 1) % 4), jnp.where(i < 4, (x + i) % 4, x)
 
     def step_a(m):
         w, yy, j = place(m)
         piece = wpiece(0, w, yy, j)
 
-        @pl.when((p == 0) & (m < 6))
+        @pl.when((p == 0) & (m >= 2) & (m < 8))
         def _():
             got(piece, SX + w * 4 + j)
 
@@ -136,7 +136,7 @@
         def _():
             copy(piece, wpiece(1, w, yy, j), ZMd, ZM + m).start()
 
-        @pl.when(m < 6)
+        @pl.when((m >= 2) & (m < 8))
         def _():
             ysend(0, w, j)
 
@@ -156,7 +156,7 @@
         def _():
             copy(piece, piece, ZMd, ZM + m).start()
 
-        @pl.when(m < 6)
+        @pl.when((m >= 2) & (m < 8))
         def _():
             ysend(1, w, j)
 
@@ -184,7 +184,7 @@
     root = p == 0
     lag_a = jnp.where(p == 3, 5, 0)
     lag_b = jnp.where(root, 20, jnp.where(p == 1, 5, 0))
-    lag_far = jnp.where(root, 28, jnp.where(p == 2, 8, 13))
+    lag_far = jnp.where(root, 28, jnp.where(p == 2, 10, 15))
 
     def yfinish(slot):
         def piece(i):
@@ -241,7 +241,7 @@
         def _():
             step_b(t - lag_b)
 
-        @pl.when(t == jnp.where(root, 14, 6))
+        @pl.when(t == jnp.where(root, 14, 8))
         def _():
             got(xblock(0, xm, crow), TP)
             copy(xblock(0, xm, crow), xblock(0, xm, crow), XP, TF).start()
@@ -254,15 +254,15 @@
         def _():
             yforward(near, t - 14)
 
-        @pl.when((p != 0) & (t >= 4) & (t < 16) & (t % 2 == 0))
-        def _():
-            yforward(near, (t - 4) // 2)
+        @pl.when((p != 0) & (t >= 6) & (t < 18) & (t % 2 == 0))
+        def _():
+            yforward(near, (t - 6) // 2)
 
         @pl.when((t >= lag_far) & (t < lag_far + 6))
         def _():
             yforward(far, t - lag_far)
 
-        @pl.when(t == jnp.where(root, 26, 13))
+        @pl.when(t == jnp.where(root, 26, 15))
         def _():
             got(xblock(1, xm, crow), TP + 1)
             pass_on(1, 3)
@@ -284,7 +284,7 @@
     act_three(far)
     partner(2)
 
-    def grads(slot, send):
+    def grads(slot, send, first=0, count=4):
         def block(i):
             yy = (y + jnp.where(i < 2, 2 - i, i + 1)) % 4
             cols = pl.ds(pl.multiple_of(yy * 512, 512), 512)
@@ -294,28 +294,25 @@
                 for j in range(4):
                     G[slot, w, yy, (j - x + 4) % 4] = part[:, j * 128 : (j + 1) * 128]
             if send:
-                for at, copies in enumerate((a_send, bp_send, bm_send)):
-
-                    @pl.when(i == at)
-                    def _(copies=copies):
-                        both(3, lambda n: copies(slot, n))
-
-        both(4, block)
+
+                @pl.when(i == 0)
+                def _():
+                    both(3, lambda n: a_send(slot, n))
+
+                @pl.when(p < 2)
+                def _():
+                    own_b(2 * i)
+                    own_b(2 * i + 1)
+
+        both(count, lambda i: block(first + i))
 
     def a_send(slot, i):
         copy(G.at[slot, 0, yo, i + 1], RY.at[slot, 0, 0, i], YPd, AY + slot * 6 + i).start()
         copy(G.at[slot, 1, yo, i + 1], RY.at[slot, 1, 0, i], YMd, AY + slot * 6 + 3 + i).start()
 
-    def bp_send(slot, i):
+    def b_send(slot, i):
         copy(G.at[slot, 1, yp, i + 1], RY.at[slot, 0, 1, i], YPd, BY + slot * 6 + i).start()
-
-    def bm_send(slot, i):
         copy(G.at[slot, 0, ym, i + 1], RY.at[slot, 1, 1, i], YMd, BY + slot * 6 + 3 + i).start()
-
-    def ab_send(slot, i):
-        a_send(slot, i)
-        bp_send(slot, i)
-        bm_send(slot, i)
 
     def add(*terms):
         total = terms[0].astype(F32)
@@ -433,14 +430,17 @@
     act(far, 2)
     grads(far, True)
 
-    @pl.when(p < 2)
-    def _():
-        both(8, own_b)
-
+    b_send(far, 0)
     act(near, 2)
-    grads(near, False)
-    both(3, lambda i: c_step(far, i))
-    both(2, lambda i: ab_send(near, i))
+    c_step(far, 0)
+    b_send(far, 1)
+    grads(near, False, 0, 2)
+    c_step(far, 1)
+    b_send(far, 2)
+    grads(near, False, 2, 2)
+    c_step(far, 2)
+    both(3, lambda i: a_send(near, i))
+    b_send(near, 0)
 
     def x_first(half):
         got(RP.at[half], XC + half)
@@ -475,10 +475,10 @@
         return jnp.where(p == 0, values[0], jnp.where(p == 1, values[1], jnp.where(p == 2, values[2], values[3])))
 
     never = 99
-    at_own_b = by_p(never, never, 1, 3)
-    at_own_a = by_p(12, 9, 6, 3)
-    at_chain_a = by_p(20, 18, 13, 10)
-    at_chain_b = by_p(never, never, never, 18)
+    at_own_b = by_p(never, never, 0, 3)
+    at_own_a = by_p(10, 7, 4, 1)
+    at_chain_a = by_p(18, 15, 12, 9)
+    at_chain_b = by_p(never, never, never, 15)
 
     def rstep(t):
         def span(start, count, body):
@@ -490,7 +490,7 @@
         span(at_own_a, 8, own_a)
         span(at_chain_b, 6, chain_b)
 
-        @pl.when(root & (t == 20))
+        @pl.when(root & (t == 18))
         def _():
             root_second()
 
@@ -506,51 +506,48 @@
             half = t // 2
             copy(S.at[1 - c, half], RP.at[half], PA, XC + half).start()
 
-        @pl.when((t == 5) | (t == 6))
-        def _():
-            x_first(t - 5)
-
-        @pl.when(t == 6)
-        def _():
-            x_send()
-
-        @pl.when(t == 8)
-        def _():
-            def piece(i):
-                y_final(far, i)
-
-                @pl.when(p < 2)
-                def _():
-                    chain_b(i * 2)
-                    chain_b(i * 2 + 1)
-
-            both(3, piece)
-
-        span(9, 2, lambda i: c_step(near, i))
-
-        @pl.when(t == 10)
-        def _():
-            ab_send(near, 2)
-
-        @pl.when(t == 12)
-        def _():
-            x_second()
-
-        @pl.when(t == 14)
-        def _():
-            c_step(near, 2)
-
-        @pl.when((t == 13) | (t == 15) | (t == 17))
-        def _():
-            i = (t - 13) // 2
-            y_final(near, i)
-
-            @pl.when(p == 2)
+        @pl.when((t == 4) | (t == 5) | (t == 7))
+        def _():
+            i = (t - 3) // 2
+            y_final(far, i)
+
+            @pl.when(p < 2)
             def _():
                 chain_b(i * 2)
                 chain_b(i * 2 + 1)
 
-    both(26, rstep)
+        @pl.when((t == 5) | (t == 6))
+        def _():
+            x_first(t - 5)
+
+        @pl.when(t == 6)
+        def _():
+            x_send()
+
+        @pl.when((t >= 8) & (t < 11))
+        def _():
+            i = t - 8
+            c_step(near, i)
+
+            @pl.when(i < 2)
+            def _():
+                b_send(near, i + 1)
+
+        @pl.when(t == 13)
+        def _():
+            x_second()
+
+        @pl.when((t == 12) | (t == 14) | (t == 16))
+        def _():
+            i = (t - 12) // 2
+            y_final(near, i)
+
+            @pl.when(p == 2)
+            def _():
+                chain_b(i * 2)
+                chain_b(i * 2 + 1)
+
+    both(24, rstep)
 
     got(XR.at[0, 1], XY + 2)
     got(XR.at[1, 1], XY + 3)

time: 108 us -> 104 us (0.963)
  the two profiles are of different devices: /device:TPU:4 before, /device:TPU:32 now
where the time goes in v4:
time: 104 us
  Pallas kernels  99.9 us (96%)
  local copies, waits for them, and re-layouts  3.53 us (3%)
    pallas_call x1, Pallas kernels, shards(): pl.pallas_call(body, out_shape=(jax.ShapeDtypeStruct((128, 2048), BF), ja...  99.9 us
    unnamed x7, local copies, waits for them, and re-layouts  3.53 us

profile of v4, /device:TPU:32, one launch (start us, length us, event | category | flops | bytes accessed | tf_op | source)
XLA Modules:
  0.0 104.1 jit_solution(5010892029983042989)
XLA Ops:
  0.6 99.9 %ffn_backward.1 = (bf16[128,2048]{1,0:T(8,128)(2,1)}, f32[128,256]{1,0:T(8,128)}, f32[256,128]{1,0:T(8,128)}) custom-call(bf16[128,2048]{1,0:T(8,128)(2,1)} %refs_0_.1, bf16[128,256]{1,0:T(8,128)(2,1)} %refs_1_.1, bf16[256,128]{1,0:T(8,128)(2,1)} %refs_2_.1, bf16[128,2048]{1,0:T(8,128)(2,1)} %refs_3_.1), custom_call_target="tpu_custom_call" | custom-call | tf_op jit(solution)/shard_map/ffn_backward/pallas_call | solution.py:647
  100.5 0.0 copy-start.1
  100.6 1.9 %copy.10 = bf16[128,2048]{1,0:T(8,128)(2,1)} copy(bf16[128,2048]{1,0:T(8,128)(2,1)} %get-tuple-element.6) | data formatting | bytes 1048576
  102.5 0.0 copy-done.1
  102.5 0.0 copy-start
  102.5 0.7 copy.11
  103.1 0.3 copy-done
  103.4 0.7 copy.12
Async XLA Ops:
  100.5 1.9 %copy-start.1 = (f32[128,256]{1,0:T(8,128)S(1)}, f32[128,256]{1,0:T(8,128)}, u32[]{:S(2)}) copy-start(f32[128,256]{1,0:T(8,128)} %get-tuple-element.7) | copy-start | bytes 393220
  102.5 1.0 copy-start

commit v5 on v4

--- a/solution.py
+++ b/solution.py
@@ -476,7 +476,7 @@
 
     never = 99
     at_own_b = by_p(never, never, 0, 3)
-    at_own_a = by_p(10, 7, 4, 1)
+    at_own_a = by_p(9, 6, 3, 0)
     at_chain_a = by_p(18, 15, 12, 9)
     at_chain_b = by_p(never, never, never, 15)
 
@@ -676,7 +676,7 @@
                 pltpu.SemaphoreType.DMA((2,)),
             ],
             compiler_params=pltpu.CompilerParams(
-                collective_id=0, has_side_effects=True, vmem_limit_bytes=60 * 2**20
+                collective_id=0, has_side_effects=True, vmem_limit_bytes=54250 * 1024
             ),
             name="ffn_backward",
         )(tokens, up_weight, down_weight, cotangent)

time: 104 us -> 102 us (0.981)
  the two profiles are of different devices: /device:TPU:32 before, /device:TPU:4 now
where the time goes in v5:
time: 102 us; the launch traced here: 100 us
  Pallas kernels  96 us (94%)
  local copies, waits for them, and re-layouts  3.78 us (4%)
    pallas_call x1, Pallas kernels, shards(): pl.pallas_call(body, out_shape=(jax.ShapeDtypeStruct((128, 2048), BF), ja...  96 us
    unnamed x7, local copies, waits for them, and re-layouts  3.78 us

profile of v5, /device:TPU:4, one launch (start us, length us, event | category | flops | bytes accessed | tf_op | source)
XLA Modules:
  0.0 100.5 jit_solution(5642126170533022169)
XLA Ops:
  0.6 0.0 copy-start
  0.6 0.8 copy-done
  1.5 0.0 copy-start.1
  1.5 0.8 copy-done.1
  2.3 96.0 %ffn_backward.1 = (bf16[128,2048]{1,0:T(8,128)(2,1)S(1)}, f32[128,256]{1,0:T(8,128)S(1)}, f32[256,128]{1,0:T(8,128)S(1)}) custom-call(bf16[128,2048]{1,0:T(8,128)(2,1)} %refs_0_.1, bf16[128,256]{1,0:T(8,128)(2,1)S(1)} %copy-done, bf16[256,128]{1,0:T(8,128)(2,1)S(1)} %copy-done.1, bf16[128,2048]{1,0:T(8,128)(2,1)} %refs_3_.1), custom_call_target="tpu_custom_call" | custom-call | tf_op jit(solution)/shard_map/ffn_backward/pallas_call | solution.py:647
  98.4 0.8 copy.10
  99.2 0.7 copy.11
  99.8 0.7 copy.12
Async XLA Ops:
  0.6 0.8 copy-start
  1.5 0.8 copy-start.1

commit v6 on v5

--- a/solution.py
+++ b/solution.py
@@ -184,7 +184,7 @@
     root = p == 0
     lag_a = jnp.where(p == 3, 5, 0)
     lag_b = jnp.where(root, 20, jnp.where(p == 1, 5, 0))
-    lag_far = jnp.where(root, 28, jnp.where(p == 2, 10, 15))
+    lag_far = jnp.where(root, 24, jnp.where(p == 2, 10, 15))
 
     def yfinish(slot):
         def piece(i):
@@ -269,7 +269,7 @@
             got(xblock(0, xp, crow), TM)
             pass_on(0, 1)
 
-        @pl.when(root & (t == 27))
+        @pl.when(root & (t == 30))
         def _():
             near_part()
 
@@ -293,22 +293,21 @@
                 part = jnp.dot(TT[slot, w], rows, preferred_element_type=F32).astype(BF)
                 for j in range(4):
                     G[slot, w, yy, (j - x + 4) % 4] = part[:, j * 128 : (j + 1) * 128]
-            if send:
-
-                @pl.when(i == 0)
-                def _():
-                    both(3, lambda n: a_send(slot, n))
-
-                @pl.when(p < 2)
-                def _():
-                    own_b(2 * i)
-                    own_b(2 * i + 1)
+                if send:
+
+                    @pl.when(p < 2)
+                    def _(w=w):
+                        own_b(2 * i + w)
+
+                    @pl.when(i == 0)
+                    def _(w=w):
+                        both(3, lambda n: a_send(slot, n, w))
 
         both(count, lambda i: block(first + i))
 
-    def a_send(slot, i):
-        copy(G.at[slot, 0, yo, i + 1], RY.at[slot, 0, 0, i], YPd, AY + slot * 6 + i).start()
-        copy(G.at[slot, 1, yo, i + 1], RY.at[slot, 1, 0, i], YMd, AY + slot * 6 + 3 + i).start()
+    def a_send(slot, i, w):
+        to = (YPd, YMd)[w]
+        copy(G.at[slot, w, yo, i + 1], RY.at[slot, w, 0, i], to, AY + slot * 6 + w * 3 + i).start()
 
     def b_send(slot, i):
         copy(G.at[slot, 1, yp, i + 1], RY.at[slot, 0, 1, i], YPd, BY + slot * 6 + i).start()
@@ -439,7 +438,8 @@
     b_send(far, 2)
     grads(near, False, 2, 2)
     c_step(far, 2)
-    both(3, lambda i: a_send(near, i))
+    for w in range(2):
+        both(3, lambda i, w=w: a_send(near, i, w))
     b_send(near, 0)
 
     def x_first(half):

time: 102 us -> 101 us (level)
  no operation moved by 1% of the time
where the time goes in v6:
time: 101 us; the launch traced here: 100 us
  Pallas kernels  95.8 us (95%)
  local copies, waits for them, and re-layouts  3.78 us (4%)
    pallas_call x1, Pallas kernels, shards(): pl.pallas_call(body, out_shape=(jax.ShapeDtypeStruct((128, 2048), BF), ja...  95.8 us
    unnamed x7, local copies, waits for them, and re-layouts  3.78 us

profile of v6, /device:TPU:4, one launch (start us, length us, event | category | flops | bytes accessed | tf_op | source)
XLA Modules:
  0.0 100.2 jit_solution(5658679806223728784)
XLA Ops:
  0.6 0.0 copy-start
  0.6 0.8 copy-done
  1.5 0.0 copy-start.1
  1.5 0.8 copy-done.1
  2.3 95.8 %ffn_backward.1 = (bf16[128,2048]{1,0:T(8,128)(2,1)S(1)}, f32[128,256]{1,0:T(8,128)S(1)}, f32[256,128]{1,0:T(8,128)S(1)}) custom-call(bf16[128,2048]{1,0:T(8,128)(2,1)} %refs_0_.1, bf16[128,256]{1,0:T(8,128)(2,1)S(1)} %copy-done, bf16[256,128]{1,0:T(8,128)(2,1)S(1)} %copy-done.1, bf16[128,2048]{1,0:T(8,128)(2,1)} %refs_3_.1), custom_call_target="tpu_custom_call" | custom-call | tf_op jit(solution)/shard_map/ffn_backward/pallas_call | solution.py:647
  98.1 0.8 copy.10
  98.9 0.7 copy.11
  99.6 0.7 copy.12
Async XLA Ops:
  0.6 0.8 copy-start
  1.5 0.8 copy-start.1
